TPU v7x, 256 devices: a whole 4x4x8 slice. The times are simulated.
256 devices in a mesh: ep: 64 (over z, y, core), tp: 4 (over x).
Axes of the slice: x: 4, y: 4, z: 8, core: 2. Of those that a mesh axis runs over, the one named last changes fastest.
Arguments:
- mixer_in: bfloat16 [24576, 2048], P(('ep', 'tp')), may hold values from -6 to 6
- expert_in: bfloat16 [24576, 2048], P(('ep', 'tp')), may hold values from -6 to 6
- mixer_gain: float32 [2048], replicated, may hold values from 0.1 to 1.9
- in_gate_weight: bfloat16 [2048, 2048], P(None, 'tp'), may hold values from -0.125 to 0.125
- out_gate_weight: bfloat16 [2048, 2048], P(None, 'tp'), may hold values from -0.125 to 0.125
- value_weight: bfloat16 [2048, 2048], P(None, 'tp'), may hold values from -0.125 to 0.125
- conv_taps: float32 [3, 2048], replicated, may hold values from -3 to 3
- mixer_proj: bfloat16 [2048, 2048], P(None, 'tp'), may hold values from -0.125 to 0.125
- expert_gain: float32 [2048], replicated, may hold values from 0.1 to 1.9
- route_ids: int32 [24576, 2], P('ep'), may hold values from 0 to 63, all different within a row; in each aligned block of 96 rows (0 to 95, 96 to 191, ...) at most 6 rows name the same one
- route_weights: float32 [24576, 2], P('ep'), may hold values from 0.1 to 1
- gate_weight: bfloat16 [64, 2048, 1024], P('ep', None, 'tp'), may hold values from -0.125 to 0.125
- up_weight: bfloat16 [64, 2048, 1024], P('ep', None, 'tp'), may hold values from -0.125 to 0.125
- down_weight: bfloat16 [64, 1024, 2048], P('ep', None, 'tp'), may hold values from -0.1875 to 0.1875
Outputs:
- mixer_out: bfloat16 [24576, 2048], P('ep', 'tp')
- expert_out: bfloat16 [24576, 2048], P('ep', 'tp')
Inputs may be any that keep to these rules, and one draw needn't show every extreme that they name: `route_ids`: each row names 2 different experts. In each aligned block of 96 rows no expert is named by more than 6 rows, a bound that some block reaches.
All inputs are finite; a program needn't handle non-finite values.
Results may differ from a plain program's by a relative error of at most 0.0076.
Values may be sent and summed in bfloat16 or wider, within the bound.
A program may use at most 64 MiB of HBM per device.

v0:
```python
import jax
import jax.numpy as jnp
from jax import lax
from jax.sharding import PartitionSpec as P

norm_eps = 1e-06


def sent_to_all(x, axis):
    peers = lax.axis_size(axis)
    return lax.all_to_all(jnp.broadcast_to(x[None], (peers, *x.shape)), axis, 0, 0, tiled=True)


def joined_along(tiles, dim):
    tiles = jnp.moveaxis(tiles, 0, dim)
    dims = tiles.shape
    return tiles.reshape(*dims[:dim], dims[dim] * dims[dim + 1], *dims[dim + 2 :])


def collect(x, axis, dim):
    tiles = sent_to_all(x, axis)
    return joined_along(tiles, dim)


def passed_along(value, axis, steps):
    count = lax.axis_size(axis)
    leading, last = (max(0, -steps), min(count, count - steps))
    return lax.ppermute(value, axis, [(source, source + steps) for source in range(leading, last)])


def rms_rows(values, gain_row):
    wide = values.astype(jnp.float32)
    scale = lax.rsqrt(jnp.mean(wide * wide, axis=-1, keepdims=True) + norm_eps)
    return (wide * scale * gain_row).astype(jnp.bfloat16)


def place_slots(route_ids, group_rows, experts, slot_cap):
    row_total, top_count = route_ids.shape
    groups = row_total // group_rows
    labels = jnp.arange(experts, dtype=jnp.int32)
    onehot = (
        route_ids.reshape(groups, group_rows * top_count)[:, :, None] == labels[None, None, :]
    ).astype(jnp.int32)
    earlier = jnp.cumsum(onehot, axis=1) - onehot
    within = jnp.sum(earlier * onehot, axis=2)
    slot_index = jnp.arange(groups, dtype=jnp.int32)[:, None] * slot_cap + within
    return slot_index.reshape(row_total, top_count)


def on_device(
    mixer_in,
    expert_in,
    mixer_gain,
    in_gate_weight,
    out_gate_weight,
    value_weight,
    conv_taps,
    mixer_proj,
    expert_gain,
    route_ids,
    route_weights,
    gate_weight,
    up_weight,
    down_weight,
):
    tok_dev = mixer_in.shape[0]
    tp_count = lax.axis_size("tp")
    ep_count = lax.axis_size("ep")
    top_count = route_ids.shape[1]
    experts = ep_count * gate_weight.shape[0]
    slot_cap = max(2, 2 * tok_dev * top_count // experts)
    tp_index = lax.axis_index("tp")
    mixer_normed = rms_rows(mixer_in, mixer_gain)
    expert_normed = rms_rows(expert_in, expert_gain)
    block_slot = place_slots(route_ids, tok_dev, experts, slot_cap)
    mixer_rows = collect(mixer_normed, "tp", 0)
    send_ids = lax.dynamic_slice_in_dim(route_ids, tp_index * tok_dev, tok_dev, 0)
    send_slot = (
        lax.dynamic_slice_in_dim(block_slot, tp_index * tok_dev, tok_dev, 0) - tp_index * slot_cap
    )
    source_count = expert_normed.shape[0]
    flat_index = (send_ids * slot_cap + send_slot).reshape(-1)
    row_table = (
        jnp.full((experts * slot_cap,), source_count, jnp.int32)
        .at[flat_index]
        .set(jnp.repeat(jnp.arange(source_count, dtype=jnp.int32), top_count))
    )
    padded_rows = jnp.concatenate(
        [expert_normed, jnp.zeros((1, expert_normed.shape[1]), jnp.bfloat16)], axis=0
    )
    outgoing = padded_rows[row_table].reshape(experts, slot_cap, expert_normed.shape[1])
    arrived = lax.all_to_all(outgoing, "ep", split_axis=0, concat_axis=0, tiled=True)
    arrived = lax.all_gather(arrived, "tp", axis=1, tiled=True)
    chan_width = in_gate_weight.shape[1]
    in_gate = jnp.dot(mixer_rows, in_gate_weight, preferred_element_type=jnp.float32)
    out_gate = jnp.dot(mixer_rows, out_gate_weight, preferred_element_type=jnp.float32)
    values = jnp.dot(mixer_rows, value_weight, preferred_element_type=jnp.float32)
    product = (in_gate * values).astype(jnp.bfloat16)
    tap_count = conv_taps.shape[0]
    rim_rows = passed_along(product[product.shape[0] - (tap_count - 1) :], "ep", 1)
    extended = jnp.concatenate([rim_rows, product], axis=0).astype(jnp.float32)
    tap_rows = lax.dynamic_slice_in_dim(conv_taps, tp_index * chan_width, chan_width, 1)
    row_count = product.shape[0]
    conv_sum = tap_rows[0] * extended[0:row_count]
    for tap_index in range(1, tap_count):
        conv_sum = conv_sum + tap_rows[tap_index] * extended[tap_index : tap_index + row_count]
    gated = (out_gate * conv_sum).astype(jnp.bfloat16)
    slots_in = arrived.reshape(-1, arrived.shape[2])
    gate_pre = jnp.dot(slots_in, gate_weight[0], preferred_element_type=jnp.float32)
    up_pre = jnp.dot(slots_in, up_weight[0], preferred_element_type=jnp.float32)
    hidden = (jax.nn.silu(gate_pre) * up_pre).astype(jnp.bfloat16)
    down_slice = down_weight[0]
    rows_part = mixer_proj
    mixer_sum = jnp.dot(
        lax.all_gather(gated, "tp", axis=1, tiled=True),
        rows_part,
        preferred_element_type=jnp.float32,
    )
    rows_part = down_slice
    expert_sum = jnp.dot(
        lax.all_gather(hidden, "tp", axis=1, tiled=True),
        rows_part,
        preferred_element_type=jnp.float32,
    )
    mixer_out = mixer_sum.astype(jnp.bfloat16)
    results = expert_sum.astype(jnp.bfloat16).reshape(ep_count, -1, expert_sum.shape[1])
    returned = lax.all_to_all(results, "ep", split_axis=0, concat_axis=0, tiled=True)
    back_index = (route_ids * (tp_count * slot_cap) + block_slot).reshape(-1)
    picked = returned.reshape(-1, returned.shape[2])[back_index].reshape(
        route_ids.shape[0], top_count, -1
    )
    shares = route_weights / jnp.sum(route_weights, axis=1, keepdims=True)
    expert_out = jnp.sum(picked.astype(jnp.float32) * shares[:, :, None], axis=1).astype(
        jnp.bfloat16
    )
    return (mixer_out, expert_out)


def solution(mesh):
    return jax.shard_map(
        on_device,
        mesh=mesh,
        in_specs=(
            P(("ep", "tp"), None),
            P(("ep", "tp"), None),
            P(),
            P(None, "tp"),
            P(None, "tp"),
            P(None, "tp"),
            P(),
            P(None, "tp"),
            P(),
            P("ep", None),
            P("ep", None),
            P("ep", None, "tp"),
            P("ep", None, "tp"),
            P("ep", None, "tp"),
        ),
        out_specs=(P("ep", "tp"), P("ep", "tp")),
        check_vma=False,
    )
```

profile of v0, /device:TPU:1, one launch (start us, length us, event | category | flops | bytes accessed | tf_op | source)
XLA Modules:
  0.0 291.8 jit_solution(16893624878074087516)
XLA Ops:
  7.2 1.0 copy.47
  8.5 2.4 reduce-window.6
  12.3 1.2 scatter_custom_fusion
  13.6 0.2 fusion.10
  14.0 3.1 %gather_fusion = bf16[384,2048]{1,0:T(8,128)(2,1)} fusion(bf16[97,2048]{1,0:T(8,128)(2,1)S(1)} %concatenate.7, s32[1024]{0:T(1024)S(1)} %pad_clamp_fusion.1), kind=kCustom, calls=%fused_computation | custom fusion | bytes 3147264 | tf_op jit(solution)/shard_map/gather | solution.py:91
  17.1 3.7 %reshape.133 = bf16[64,6,2048]{2,1,0:T(8,128)(2,1)} reshape(bf16[384,2048]{1,0:T(8,128)(2,1)} %gather_fusion) | data formatting | bytes 3145728 | tf_op jit(solution)/shard_map/reshape | solution.py:91
  20.8 62.8 %all_to_all.15 = bf16[64,6,2048]{2,1,0:T(8,128)(2,1)S(1)} all-to-all(bf16[64,6,2048]{2,1,0:T(8,128)(2,1)} %reshape.133), channel_id=1, replica_groups=mesh['ep'=64,'tp'=4] {'ep'}, dimensions={0} | all-to-all | bytes 3145728 | tf_op jit(solution)/shard_map/all_to_all | solution.py:92
  83.6 2.0 copy.54
  85.7 0.2 all-gather.8.cloned.1.call-start
  85.9 65.5 %all-gather.6.cloned.1.call-done = bf16[64,24,2048]{2,0,1:T(8,128)(2,1)} async-done(((bf16[64,6,2048]{2,0,1:T(8,128)(2,1)}), bf16[64,24,2048]{2,0,1:T(8,128)(2,1)}) %all-gather.6.cloned.1.call-update) | async-done | bytes 6291472 | tf_op jit(solution)/shard_map/all_gather | solution.py:93
  151.4 6.2 %copy.55 = bf16[64,24,2048]{2,1,0:T(8,128)(2,1)S(1)} copy(bf16[64,24,2048]{2,0,1:T(8,128)(2,1)} %all-gather.6.cloned.1.call-done) | data formatting | bytes 12582912 | tf_op jit(solution)/shard_map/all_gather | solution.py:93
  157.7 3.2 %fusion.5 = f32[1536,256]{1,0:T(8,128)S(1)} fusion(bf16[1536,2048]{1,0:T(8,128)(2,1)S(1)} %bitcast.43, bf16[1,2048,256]{2,1,0:T(8,128)(2,1)} %param.25), kind=kOutput, calls=%fused_computation.14 | convolution fusion | flops 1610612736 | bytes 8912896 | tf_op jit(solution)/shard_map/dot_general | solution.py:109
  160.9 3.0 %fusion = bf16[1536,256]{1,0:T(8,128)(2,1)} fusion(bf16[1536,2048]{1,0:T(8,128)(2,1)S(1)} %bitcast.44, f32[1536,256]{1,0:T(8,128)S(1)} %fusion.5, bf16[1,2048,256]{2,1,0:T(8,128)(2,1)S(1)} %copy-done.8), kind=kOutput, calls=%fused_computation.5 | convolution fusion | flops 1612972032 | bytes 9699328 | tf_op jit(solution)/shard_map/dot_general | solution.py:110
  163.9 0.2 fusion.7
  164.3 1.4 broadcast_in_dim.8
  165.6 4.3 %all-to-all-start = ((bf16[4,96,2048]{2,1,0:T(8,128)(2,1)}), bf16[4,96,2048]{2,1,0:T(8,128)(2,1)}, u32[]{:S(2)}, u32[]{:S(2)}) async-start(bf16[4,96,2048]{2,1,0:T(8,128)(2,1)} %broadcast_in_dim.8), calls=%async_computation | async-start | bytes 3145728 | tf_op jit(solution)/shard_map/all_to_all | solution.py:11
  170.0 28.0 %all-to-all-done = bf16[4,96,2048]{2,1,0:T(8,128)(2,1)} async-done(((bf16[4,96,2048]{2,1,0:T(8,128)(2,1)}), bf16[4,96,2048]{2,1,0:T(8,128)(2,1)}, u32[]{:S(2)}, u32[]{:S(2)}) %all-to-all-start) | async-done | bytes 1572896 | tf_op jit(solution)/shard_map/all_to_all | solution.py:11
  198.0 2.5 fusion.22
  200.6 2.4 fusion.2
  203.0 5.1 %collective-permute-start = (bf16[2,512]{1,0:T(2,128)(2,1)S(1)}, bf16[2,512]{1,0:T(2,128)(2,1)S(1)}, u32[]{:S(2)}, u32[]{:S(2)}) collective-permute-start(bf16[2,512]{1,0:T(2,128)(2,1)S(1)} %slice.44), channel_id=1, source_target_pairs={{0,4},{4,8},{8,12},{12,16},{16,20},{20,24},{24,28},{28,32},{32,36}... | collective-permute-start | bytes 6152 | tf_op jit(solution)/shard_map/ppermute | solution.py:28
  208.2 0.9 constant_dynamic-slice_fusion
  209.2 8.7 %all-gather.8.cloned.1.call-done = bf16[1536,1024]{1,0:T(8,128)(2,1)} async-done(((bf16[1536,256]{1,0:T(8,128)(2,1)}), bf16[1536,1024]{1,0:T(8,128)(2,1)}) %all-gather.8.cloned.1.call-update) | async-done | bytes 3145744 | tf_op jit(solution)/shard_map/all_gather | solution.py:121
  217.8 5.1 %convolution_convert_fusion = bf16[1536,512]{1,0:T(8,128)(2,1)} fusion(bf16[1536,1024]{1,0:T(8,128)(2,1)} %all-gather.8.cloned.1.call-done, bf16[1,1024,512]{2,1,0:T(8,128)(2,1)} %param.27), kind=kOutput, calls=%fused_computation.3 | convolution fusion | flops 1611399168 | bytes 5767168 | tf_op jit(solution)/shard_map/dot_general | solution.py:120
  223.0 12.5 %all-to-all-start.2 = ((bf16[64,24,512]{2,1,0:T(8,128)(2,1)}), bf16[64,24,512]{2,1,0:T(8,128)(2,1)}, u32[]{:S(2)}, u32[]{:S(2)}) async-start(bf16[64,24,512]{2,1,0:T(8,128)(2,1)} %bitcast.45), calls=%async_computation.2 | async-start | bytes 3145728 | tf_op jit(solution)/shard_map/all_to_all | solution.py:127
  235.5 0.3 all-gather.4.cloned.1.call-start
  235.7 3.9 %fusion.1 = bf16[384,512]{1,0:T(8,128)(2,1)} fusion(bf16[384,2048]{1,0:T(8,128)(2,1)} %bitcast, bf16[2048,512]{1,0:T(8,128)(2,1)} %param.18, f32[386,512]{1,0:T(8,128)S(1)} %maximum_convert_fusion, f32[512]{0:T(512)S(1)} %bitcast.48, f32[512]{0:T(512)S(1)} %bitcast.47, f32[512]{0:T(512)S(1)} %bitcast.46), kind=kOutput, calls=%fused_computation.9 | convolution fusion | flops 806682624 | bytes 6428672 | tf_op jit(solution)/shard_map/dot_general | solution.py:96
  240.2 28.4 %all-gather.4.cloned.1.call-done = bf16[384,2048]{1,0:T(8,128)(2,1)} async-done(((bf16[384,512]{1,0:T(8,128)(2,1)}), bf16[384,2048]{1,0:T(8,128)(2,1)}) %all-gather.4.cloned.1.call-update) | async-done | bytes 1572880 | tf_op jit(solution)/shard_map/all_gather | solution.py:115
  268.6 3.8 %convolution_convert_fusion.1 = bf16[384,512]{1,0:T(8,128)(2,1)} fusion(bf16[384,2048]{1,0:T(8,128)(2,1)} %all-gather.4.cloned.1.call-done, bf16[2048,512]{1,0:T(8,128)(2,1)} %param.21), kind=kOutput, calls=%fused_computation.11 | convolution fusion | flops 805502976 | bytes 4063232 | tf_op jit(solution)/shard_map/dot_general | solution.py:114
  272.4 2.1 all-to-all-done.2
  274.5 4.3 %gather_fusion.1 = bf16[768,512]{1,0:T(8,128)(2,1)S(1)} fusion(bf16[1536,512]{1,0:T(8,128)(2,1)} %bitcast.12, s32[1024]{0:T(1024)S(1)} %pad_clamp_fusion), kind=kCustom, calls=%fused_computation.1 | custom fusion | bytes 1575936 | tf_op jit(solution)/shard_map/gather | solution.py:129
  278.8 2.1 reshape.139
  280.9 4.3 %multiply_reduce_fusion = bf16[384,512]{1,0:T(8,128)(2,1)} fusion(f32[384,2,512]{2,1,0:T(2,128)} %reshape.139, f32[384,2]{1,0:T(8,128)S(1)} %copy.57), kind=kLoop, calls=%fused_computation.6 | loop fusion | flops 589824 | bytes 1969152 | tf_op jit(solution)/shard_map/reduce_sum | solution.py:133
  (61 shorter events, 2.8 us)
Async XLA Ops:
  7.2 190.8 %copy-start = (bf16[2048,512]{1,0:T(8,128)(2,1)S(1)}, bf16[2048,512]{1,0:T(8,128)(2,1)}, u32[]{:S(2)}) copy-start(bf16[2048,512]{1,0:T(8,128)(2,1)} %param.17) | copy-start | bytes 6291460
  7.2 144.2 %all-gather.6.cloned.1.call-start = ((), (), s32[]{:S(2)}) async-start(), calls=%async_computation.4 | async-start | bytes 7864320 | tf_op jit(solution)/shard_map/all_gather | solution.py:93
  8.2 3.6 %copy-start.3 = (s32[384,2]{0,1:T(2,128)S(1)}, s32[384,2]{0,1:T(2,128)}, u32[]{:S(2)}) copy-start(s32[384,2]{0,1:T(2,128)} %param.23) | copy-start | bytes 9220
  8.4 5.1 %copy-start.1 = (bf16[96,2048]{1,0:T(8,128)(2,1)S(1)}, bf16[96,2048]{1,0:T(8,128)(2,1)}, u32[]{:S(2)}) copy-start(bf16[96,2048]{1,0:T(8,128)(2,1)} %param.15) | copy-start | bytes 1179652
  8.5 5.3 %copy-start.5 = (f32[2048]{0:T(1024)S(1)}, f32[2048]{0:T(1024)}, u32[]{:S(2)}) copy-start(f32[2048]{0:T(1024)} %param.22) | copy-start | bytes 24580
  85.7 132.2 %all-gather.8.cloned.1.call-start = ((), (), s32[]{:S(2)}) async-start(), calls=%async_computation.5 | async-start | bytes 3932160 | tf_op jit(solution)/shard_map/all_gather | solution.py:121
  157.6 3.2 %copy-start.8 = (bf16[1,2048,256]{2,1,0:T(8,128)(2,1)S(1)}, bf16[1,2048,256]{2,1,0:T(8,128)(2,1)}, u32[]{:S(2)}) copy-start(bf16[1,2048,256]{2,1,0:T(8,128)(2,1)} %param.26) | copy-start | bytes 3145732
  160.9 3.0 %copy-start.2 = (bf16[96,2048]{1,0:T(8,128)(2,1)S(1)}, bf16[96,2048]{1,0:T(8,128)(2,1)}, u32[]{:S(2)}) copy-start(bf16[96,2048]{1,0:T(8,128)(2,1)} %param.14) | copy-start | bytes 1179652
  160.9 3.2 %copy-start.6 = (f32[2048]{0:T(1024)S(1)}, f32[2048]{0:T(1024)}, u32[]{:S(2)}) copy-start(f32[2048]{0:T(1024)} %param.16) | copy-start | bytes 24580
  165.6 32.4 %all-to-all-start = ((bf16[4,96,2048]{2,1,0:T(8,128)(2,1)}), bf16[4,96,2048]{2,1,0:T(8,128)(2,1)}, u32[]{:S(2)}, u32[]{:S(2)}) async-start(bf16[4,96,2048]{2,1,0:T(8,128)(2,1)} %broadcast_in_dim.8), calls=%async_computation | async-start | bytes 3145728 | tf_op jit(solution)/shard_map/all_to_all | solution.py:11
  198.0 2.6 copy-start.7
  203.0 6.0 %collective-permute-start = (bf16[2,512]{1,0:T(2,128)(2,1)S(1)}, bf16[2,512]{1,0:T(2,128)(2,1)S(1)}, u32[]{:S(2)}, u32[]{:S(2)}) collective-permute-start(bf16[2,512]{1,0:T(2,128)(2,1)S(1)} %slice.44), channel_id=1, source_target_pairs={{0,4},{4,8},{8,12},{12,16},{16,20},{20,24},{24,28},{28,32},{32,36}... | collective-permute-start | bytes 6152 | tf_op jit(solution)/shard_map/ppermute | solution.py:28
  223.0 51.5 %all-to-all-start.2 = ((bf16[64,24,512]{2,1,0:T(8,128)(2,1)}), bf16[64,24,512]{2,1,0:T(8,128)(2,1)}, u32[]{:S(2)}, u32[]{:S(2)}) async-start(bf16[64,24,512]{2,1,0:T(8,128)(2,1)} %bitcast.45), calls=%async_computation.2 | async-start | bytes 3145728 | tf_op jit(solution)/shard_map/all_to_all | solution.py:127
  235.5 33.1 %all-gather.4.cloned.1.call-start = ((), (), s32[]{:S(2)}) async-start(), calls=%async_computation.3 | async-start | bytes 1966080 | tf_op jit(solution)/shard_map/all_gather | solution.py:115
  235.7 4.2 %copy-start.4 = (f32[384,2]{0,1:T(2,128)S(1)}, f32[384,2]{0,1:T(2,128)}, u32[]{:S(2)}) copy-start(f32[384,2]{0,1:T(2,128)} %param.24) | copy-start | bytes 9220
Sparse Core Ops, SparseCore 0:
  85.8 65.5 all-gather.5
  164.0 53.7 all-gather.7
  239.8 28.7 all-gather.3
where the time goes:
time: 292 us
  waiting for transfers between devices  133 us (46%)
  blocking collectives  62.8 us (22%)
  local copies, waits for them, and re-layouts  27.6 us (9%)
  matrix products  24 us (8%)
  starting transfers between devices  22.4 us (8%)
  between operations  14.1 us (5%)
  other arithmetic  8 us (3%)
    all_gather x1, waiting for transfers between devices, on_device(): arrived = lax.all_gather(arrived, 'tp', axis=1, tiled=True)  65.5 us
    all_to_all x1, blocking collectives, on_device(): lax.all_to_all(outgoing, 'ep', split_axis=0, concat_axis=0, tiled=True)  62.8 us
    all_gather x1, waiting for transfers between devices, on_device(): lax.all_gather(gated, 'tp', axis=1, tiled=True)  28.4 us
    all_to_all x1, waiting for transfers between devices, sent_to_all(): lax.all_to_all(jnp.broadcast_to(x[None], (peers, *x.shape)), axis, 0, 0,...  28 us
    all_to_all x1, starting transfers between devices, on_device(): lax.all_to_all(results, 'ep', split_axis=0, concat_axis=0, tiled=True)  12.5 us
    all_gather x1, waiting for transfers between devices, on_device(): lax.all_gather(hidden, 'tp', axis=1, tiled=True)  8.66 us
    all_gather x1, local copies, waits for them, and re-layouts, on_device(): arrived = lax.all_gather(arrived, 'tp', axis=1, tiled=True)  6.23 us
  transfers between devices with their start and end apart: 6, of which 5 were waited for; matrix products, arithmetic and copies ran while one was open for 5% of the time, Pallas kernels for 0%

commit v1 on v0

v1 whole, which is shorter than its diff:
```python
import jax
import jax.numpy as jnp
from jax import lax
from jax.experimental import pallas as pl
from jax.experimental.pallas import tpu as pltpu
from jax.sharding import PartitionSpec as P

norm_eps = 1e-06
Z, Y, C, X = 8, 4, 2, 4
PLANE = Y * C
EP = Z * PLANE
CAP = 24
MESH = pl.DeviceIdType.MESH


def rms_rows(values, gain_row):
    wide = values.astype(jnp.float32)
    scale = lax.rsqrt(jnp.mean(wide * wide, axis=-1, keepdims=True) + norm_eps)
    return (wide * scale * gain_row).astype(jnp.bfloat16)


def offset_of(step):
    forth, back = 1 + step // 2, Z - (step + 1) // 2
    dz = jnp.where(lax.rem(step, 2) == 0, forth, back)
    return jnp.where(step == Z - 1, 0, dz)


def kernel(
    mixer_in, expert_in, mixer_gain, expert_gain, taps, ids, weights,
    wi_hbm, wo_hbm, wv_hbm, wp_hbm, wg_hbm, wu_hbm, wd_hbm,
    mixer_out, expert_out,
    wi, wo, wv, wp, wg, wu, wd,
    tok_send, tok, mrows, send, rows, hid, res, ret, gat, ext, ogate, acc, rim_s, rim_r, slot_rows, cols,
    load_sem, tok_ss, tok_rs, mix_ss, mix_rs, disp_ss, disp_rs, row_ss, row_rs, hid_ss, hid_rs,
    ret_ss, ret_rs, gat_ss, gat_rs, rim_ss, rim_rs,
):
    ep, tp = lax.axis_index("ep"), lax.axis_index("tp")
    z = ep // PLANE
    right, left, far = lax.rem(tp + 1, X), lax.rem(tp + 3, X), lax.rem(tp + 2, X)

    loads = [
        pltpu.make_async_copy(src, dst, load_sem.at[i])
        for i, (src, dst) in enumerate(
            ((wi_hbm, wi), (wo_hbm, wo), (wv_hbm, wv), (wg_hbm, wg), (wu_hbm, wu), (wd_hbm, wd), (wp_hbm, wp))
        )
    ]
    for load in loads:
        load.start()

    barrier = pltpu.get_barrier_semaphore()

    @pl.loop(1, EP)
    def _(d):
        pl.semaphore_signal(barrier, inc=1, device_id={"ep": lax.rem(ep + d, EP)}, device_id_type=MESH)

    for other in (right, left, far):
        pl.semaphore_signal(barrier, inc=1, device_id={"tp": other}, device_id_type=MESH)

    def to_ep(src, dst, ss, rs, target):
        return pltpu.make_async_remote_copy(src, dst, ss, rs, device_id={"ep": target}, device_id_type=MESH)

    def to_tp(src, dst, ss, rs, target):
        return pltpu.make_async_remote_copy(src, dst, ss, rs, device_id={"tp": target}, device_id_type=MESH)

    def await_recv(ref, sem):
        to_tp(ref, ref, sem, sem, right).wait_recv()

    def await_send(ref, sem):
        to_tp(ref, ref, sem, sem, right).wait_send()

    normed = rms_rows(expert_in[...], expert_gain[...])
    for k in range(X):
        tok_send[k] = normed[:, k * 512 : (k + 1) * 512]
    mrows[tp] = rms_rows(mixer_in[...], mixer_gain[...])
    tok[tp] = tok_send[tp]

    pl.semaphore_wait(barrier, EP + 2)

    for i, other in enumerate((right, left, far)):
        to_tp(tok_send.at[other], tok.at[tp], tok_ss, tok_rs, other).start()
    to_tp(mrows.at[tp], mrows.at[tp], mix_ss.at[0], mix_rs.at[0], right).start()
    to_tp(mrows.at[tp], mrows.at[tp], mix_ss.at[1], mix_rs.at[1], left).start()

    count = ids.shape[1]
    labels = lax.broadcasted_iota(jnp.int32, (EP, count), 0)
    hot = [ids[k : k + 1, :] == labels for k in range(2)]
    named = jnp.where(hot[0] | hot[1], 1.0, 0.0).astype(jnp.bfloat16)
    older = (
        lax.broadcasted_iota(jnp.int32, (count, count), 0) < lax.broadcasted_iota(jnp.int32, (count, count), 1)
    )
    earlier = jnp.dot(named, jnp.where(older, 1.0, 0.0).astype(jnp.bfloat16), preferred_element_type=jnp.float32)
    total = weights[0:1, :] + weights[1:2, :]
    for k in range(2):
        within = jnp.sum(jnp.where(hot[k], earlier, 0.0), axis=0, keepdims=True)
        slot = ids[k : k + 1, :].astype(jnp.float32) * CAP + within
        slot_rows[k : k + 1, :] = slot
        cols[k] = jnp.transpose(jnp.broadcast_to(slot, (128, count)))
        cols[2 + k] = jnp.transpose(jnp.broadcast_to(weights[k : k + 1, :] / total, (128, count)))

    await_recv(tok.at[pl.ds(0, 3)], tok_rs)

    @pl.loop(0, Z)
    def _(step):
        plane = lax.rem(z + offset_of(step), Z)
        index = (lax.broadcasted_iota(jnp.int32, (PLANE * CAP, count), 0) + plane * (PLANE * CAP)).astype(jnp.float32)
        pick = (index == slot_rows[0:1, :]) | (index == slot_rows[1:2, :])
        moved = jnp.dot(
            jnp.where(pick, 1.0, 0.0).astype(jnp.bfloat16),
            tok[...].reshape(count, 512),
            preferred_element_type=jnp.float32,
        )
        send[pl.ds(plane * PLANE, PLANE)] = moved.reshape(PLANE, CAP, 512).astype(jnp.bfloat16)

        @pl.loop(0, PLANE)
        def _(j):
            target = plane * PLANE + j

            @pl.when(target != ep)
            def _():
                to_ep(send.at[target], rows.at[tp, ep], disp_ss, disp_rs.at[step], target).start()

            @pl.when(target == ep)
            def _():
                rows[tp, ep] = send[ep]

    half = mrows.shape[1] // 2
    await_recv(mrows.at[left], mix_rs.at[0])
    piece = mrows.at[left, pl.ds(0, half)]
    to_tp(piece, piece, mix_ss.at[2], mix_rs.at[2], right).start()
    await_recv(mrows.at[right], mix_rs.at[1])
    piece = mrows.at[right, pl.ds(half, half)]
    to_tp(piece, piece, mix_ss.at[2], mix_rs.at[3], left).start()

    def ring_send(buf, ss, rs, plane, step):
        block = buf.at[tp, pl.ds(plane * PLANE, PLANE)]
        to_tp(block, block, ss.at[0], rs.at[0, step], right).start()
        to_tp(block, block, ss.at[1], rs.at[1, step], left).start()

    def ring_pass(buf, ss, rs, plane, step):
        await_recv(buf.at[left, pl.ds(plane * PLANE, PLANE)], rs.at[0, step])
        block = buf.at[left, pl.ds(plane * PLANE, PLANE // 2)]
        to_tp(block, block, ss.at[2], rs.at[2, step], right).start()
        await_recv(buf.at[right, pl.ds(plane * PLANE, PLANE)], rs.at[1, step])
        block = buf.at[right, pl.ds(plane * PLANE + PLANE // 2, PLANE // 2)]
        to_tp(block, block, ss.at[2], rs.at[3, step], left).start()

    def ring_end(buf, rs, plane, step):
        await_recv(buf.at[far, pl.ds(plane * PLANE, PLANE // 2)], rs.at[2, step])
        await_recv(buf.at[far, pl.ds(plane * PLANE + PLANE // 2, PLANE // 2)], rs.at[3, step])

    def source_plane(step):
        return lax.rem(z + Z - offset_of(step), Z)

    def await_plane(buf, plane, sem, step):
        @pl.when(step == Z - 1)
        def _():
            await_recv(buf.at[pl.ds(plane * PLANE, PLANE - 1)], sem.at[step])

        @pl.when(step != Z - 1)
        def _():
            await_recv(buf.at[pl.ds(plane * PLANE, PLANE)], sem.at[step])

    def stage_rows(step):
        plane = source_plane(step)
        await_plane(rows.at[tp], plane, disp_rs, step)
        ring_send(rows, row_ss, row_rs, plane, step)

    def stage_gate_up(step):
        plane = source_plane(step)
        ring_end(rows, row_rs, plane, step)
        gate = up = None
        for k in range(X):
            x = rows[k, pl.ds(plane * PLANE, PLANE)].reshape(PLANE * CAP, 512)
            g = jnp.dot(x, wg[k * 512 : (k + 1) * 512, :], preferred_element_type=jnp.float32)
            u = jnp.dot(x, wu[k * 512 : (k + 1) * 512, :], preferred_element_type=jnp.float32)
            gate, up = (g, u) if k == 0 else (gate + g, up + u)
        h = gate / (1.0 + jnp.exp(-gate)) * up
        hid[tp, pl.ds(plane * PLANE, PLANE)] = h.reshape(PLANE, CAP, 256).astype(jnp.bfloat16)
        ring_send(hid, hid_ss, hid_rs, plane, step)

    def stage_down(step):
        plane = source_plane(step)
        ring_end(hid, hid_rs, plane, step)
        out = None
        for k in range(X):
            h = hid[k, pl.ds(plane * PLANE, PLANE)].reshape(PLANE * CAP, 256)
            o = jnp.dot(h, wd[k * 256 : (k + 1) * 256, :], preferred_element_type=jnp.float32)
            out = o if k == 0 else out + o
        res[pl.ds(plane * PLANE, PLANE)] = out.reshape(PLANE, CAP, 512).astype(jnp.bfloat16)

        @pl.loop(0, PLANE)
        def _(j):
            target = plane * PLANE + j

            @pl.when(target != ep)
            def _():
                to_ep(res.at[target], ret.at[ep], ret_ss, ret_rs.at[step], target).start()

            @pl.when(target == ep)
            def _():
                ret[ep] = res[ep]

    def stage_combine(step):
        plane = lax.rem(z + offset_of(step), Z)
        await_plane(ret, plane, ret_rs, step)
        index = lax.broadcasted_iota(jnp.int32, (count, PLANE * CAP), 1) + plane * (PLANE * CAP)
        index = index.astype(jnp.float32)
        share = jnp.where(cols[0][:, 0:1] == index, cols[2][:, 0:1], 0.0)
        share = jnp.where(cols[1][:, 0:1] == index, cols[3][:, 0:1], share)
        high = share.astype(jnp.bfloat16)
        low = (share - high.astype(jnp.float32)).astype(jnp.bfloat16)
        got = ret[pl.ds(plane * PLANE, PLANE)].reshape(PLANE * CAP, 512)
        acc[...] += jnp.dot(high, got, preferred_element_type=jnp.float32) + jnp.dot(
            low, got, preferred_element_type=jnp.float32
        )

    acc[...] = jnp.zeros(acc.shape, jnp.float32)
    for load in loads[:3]:
        load.wait()
    stage_rows(0)
    stage_rows(1)

    await_recv(mrows.at[far, pl.ds(0, half)], mix_rs.at[2])
    await_recv(mrows.at[far, pl.ds(half, half)], mix_rs.at[3])

    @pl.loop(0, 2)
    def _(n):
        span = pl.ds(pl.multiple_of(n * 256, 256), 256)
        m = mrows[...].reshape(count, 2048)
        in_gate = jnp.dot(m, wi[:, span], preferred_element_type=jnp.float32)
        values = jnp.dot(m, wv[:, span], preferred_element_type=jnp.float32)
        product = (in_gate * values).astype(jnp.bfloat16)
        ext[8:, span] = product.astype(jnp.float32)
        rim_s[:, span] = product[count - 16 :]
        ogate[:, span] = jnp.dot(m, wo[:, span], preferred_element_type=jnp.float32)

    to_ep(rim_s, rim_r, rim_ss, rim_rs, lax.rem(ep + 1, EP)).start()
    for load in loads[3:]:
        load.wait()

    def stage_gated():
        await_recv(rim_r, rim_rs)
        before = rim_r[...].astype(jnp.float32)[8:]
        ext[0:8, :] = jnp.where(ep == 0, jnp.zeros_like(before), before)

        @pl.loop(0, 4)
        def _(n):
            span = pl.ds(pl.multiple_of(n * 128, 128), 128)
            tap_span = pl.ds(pl.multiple_of(tp * 512 + n * 128, 128), 128)
            conv = taps[0:1, tap_span] * ext[6 : 6 + count, span]
            conv = conv + taps[1:2, tap_span] * ext[7 : 7 + count, span]
            conv = conv + taps[2:3, tap_span] * ext[8 : 8 + count, span]
            gat[tp, :, span] = (ogate[:, span] * conv).astype(jnp.bfloat16)

    @pl.loop(2, Z + 5)
    def _(s):
        @pl.when(s < Z)
        def _():
            stage_rows(s)

        @pl.when(s < Z + 2)
        def _():
            ring_pass(rows, row_ss, row_rs, source_plane(s - 2), s - 2)

        @pl.when((s >= 3) & (s < Z + 3))
        def _():
            stage_gate_up(s - 3)

        @pl.when((s >= 4) & (s < Z + 4))
        def _():
            ring_pass(hid, hid_ss, hid_rs, source_plane(s - 4), s - 4)

        @pl.when(s >= 5)
        def _():
            stage_down(s - 5)

        @pl.when(s == 4)
        def _():
            stage_gated()

        @pl.when(s == Z + 3)
        def _():
            to_tp(gat.at[tp], gat.at[tp], gat_ss.at[0], gat_rs.at[0], right).start()
            to_tp(gat.at[tp], gat.at[tp], gat_ss.at[1], gat_rs.at[1], left).start()

        @pl.when(s >= 7)
        def _():
            stage_combine(s - 7)

    half_g = count // 2
    await_recv(gat.at[left], gat_rs.at[0])
    piece = gat.at[left, pl.ds(0, half_g)]
    to_tp(piece, piece, gat_ss.at[2], gat_rs.at[2], right).start()
    await_recv(gat.at[right], gat_rs.at[1])
    piece = gat.at[right, pl.ds(half_g, half_g)]
    to_tp(piece, piece, gat_ss.at[2], gat_rs.at[3], left).start()
    stage_combine(Z - 2)
    stage_combine(Z - 1)
    expert_out[...] = acc[...].astype(jnp.bfloat16)
    await_recv(gat.at[far, pl.ds(0, half_g)], gat_rs.at[2])
    await_recv(gat.at[far, pl.ds(half_g, half_g)], gat_rs.at[3])

    @pl.loop(0, 2)
    def _(n):
        span = pl.ds(pl.multiple_of(n * 256, 256), 256)
        out = None
        for k in range(X):
            o = jnp.dot(gat[k], wp[k * 512 : (k + 1) * 512, span], preferred_element_type=jnp.float32)
            out = o if k == 0 else out + o
        mixer_out[:, span] = out.astype(jnp.bfloat16)

    await_send(tok.at[pl.ds(0, 3)], tok_ss)
    await_send(send.at[pl.ds(0, EP - 1)], disp_ss)
    await_send(res.at[pl.ds(0, EP - 1)], ret_ss)
    await_send(rim_s, rim_ss)
    for buf, sem in ((mrows, mix_ss), (rows, row_ss), (hid, hid_ss), (gat, gat_ss)):
        for i in range(3):
            await_send(buf.at[0], sem.at[i])


def on_device(
    mixer_in, expert_in, mixer_gain, in_gate_weight, out_gate_weight, value_weight, conv_taps, mixer_proj,
    expert_gain, route_ids, route_weights, gate_weight, up_weight, down_weight,
):
    bf16, f32 = jnp.bfloat16, jnp.float32
    own, wide = mixer_in.shape
    count = route_ids.shape[0]
    local = pl.BlockSpec(memory_space=pltpu.VMEM)
    remote = pl.BlockSpec(memory_space=pl.ANY)
    dma, vmem = pltpu.SemaphoreType.DMA, pltpu.VMEM
    out = jax.ShapeDtypeStruct((count, 512), bf16)
    return pl.pallas_call(
        kernel,
        out_shape=(out, out),
        in_specs=[local] * 7 + [remote] * 7,
        out_specs=(local, local),
        scratch_shapes=[
            *[vmem((wide, 512), bf16)] * 4, *[vmem((wide, 256), bf16)] * 2, vmem((1024, 512), bf16),
            vmem((X, own, 512), bf16), vmem((X, own, 512), bf16), vmem((X, own, wide), bf16),
            vmem((EP, CAP, 512), bf16), vmem((X, EP, CAP, 512), bf16), vmem((X, EP, CAP, 256), bf16),
            vmem((EP, CAP, 512), bf16), vmem((EP, CAP, 512), bf16), vmem((X, count, 512), bf16),
            vmem((count + 8, 512), f32), vmem((count, 512), f32), vmem((count, 512), f32),
            vmem((16, 512), bf16), vmem((16, 512), bf16), vmem((8, count), f32), vmem((4, count, 128), f32),
            dma((7,)), dma, dma, dma((3,)), dma((4,)), dma, dma((Z,)), dma((3,)), dma((4, Z)), dma((3,)), dma((4, Z)),
            dma, dma((Z,)), dma((3,)), dma((4,)), dma, dma,
        ],
        compiler_params=pltpu.CompilerParams(
            collective_id=0, has_side_effects=True, vmem_limit_bytes=62 * 2**20
        ),
        name="mixer_and_experts",
    )(
        mixer_in, expert_in, mixer_gain.reshape(1, -1), expert_gain.reshape(1, -1), conv_taps,
        route_ids.T, route_weights.T,
        in_gate_weight, out_gate_weight, value_weight, mixer_proj, gate_weight[0], up_weight[0], down_weight[0],
    )


def solution(mesh):
    return jax.shard_map(
        on_device,
        mesh=mesh,
        in_specs=(
            P(("ep", "tp"), None),
            P(("ep", "tp"), None),
            P(),
            P(None, "tp"),
            P(None, "tp"),
            P(None, "tp"),
            P(),
            P(None, "tp"),
            P(),
            P("ep", None),
            P("ep", None),
            P("ep", None, "tp"),
            P("ep", None, "tp"),
            P("ep", None, "tp"),
        ),
        out_specs=(P("ep", "tp"), P("ep", "tp")),
        check_vma=False,
    )
```

time: 292 us -> 138 us (0.47)
  the two profiles are of different devices: /device:TPU:1 before, /device:TPU:25 now
where the time goes in v1:
time: 138 us
  Pallas kernels  134 us (97%)
  local copies, waits for them, and re-layouts  3.53 us (3%)
    pallas_call x1, Pallas kernels, on_device(): pl.pallas_call(kernel, out_shape=(out, out), in_specs=[local] * 7 + [remo...  134 us
    unnamed x2, local copies, waits for them, and re-layouts  3.53 us

profile of v1, /device:TPU:25, one launch (start us, length us, event | category | flops | bytes accessed | tf_op | source)
XLA Modules:
  0.0 137.8 jit_solution(14235110427318118971)
XLA Ops:
  0.6 133.6 %mixer_and_experts.1 = (bf16[384,512]{1,0:T(8,128)(2,1)}, bf16[384,512]{1,0:T(8,128)(2,1)}) custom-call(bf16[96,2048]{1,0:T(8,128)(2,1)} %mixer_in.1, bf16[96,2048]{1,0:T(8,128)(2,1)} %expert_in.1, f32[1,2048]{1,0:T(1,128)} %bitcast.10, f32[1,2048]{1,0:T(1,128)} %bitcast.11, f32[3,2048]{1,0:T(4,128)} %taps.1, s32[2,384]{1,0:T(2,128)} %bitcast.12, ...), custom_call_target="tpu_custom_call" | custom-call | tf_op jit(solution)/shard_map/mixer_and_experts/pallas_call | solution.py:332
  134.2 1.8 %copy.18 = bf16[384,512]{1,0:T(8,128)(2,1)} copy(bf16[384,512]{1,0:T(8,128)(2,1)} %get-tuple-element.4) | data formatting | bytes 786432
  136.0 1.8 %copy.19 = bf16[384,512]{1,0:T(8,128)(2,1)} copy(bf16[384,512]{1,0:T(8,128)(2,1)} %get-tuple-element.5) | data formatting | bytes 786432

commit v2 on v1

--- a/solution.py
+++ b/solution.py
@@ -10,6 +10,9 @@
 PLANE = Y * C
 EP = Z * PLANE
 CAP = 24
+ORDER = (2, 6, 3, 5, 4, 1, 7, 0)
+LAG = 10
+FAR = 5
 MESH = pl.DeviceIdType.MESH
 
 
@@ -20,9 +23,10 @@
 
 
 def offset_of(step):
-    forth, back = 1 + step // 2, Z - (step + 1) // 2
-    dz = jnp.where(lax.rem(step, 2) == 0, forth, back)
-    return jnp.where(step == Z - 1, 0, dz)
+    dz = 0
+    for at, offset in enumerate(ORDER):
+        dz = jnp.where(step == at, offset, dz)
+    return dz
 
 
 def kernel(
@@ -30,8 +34,8 @@
     wi_hbm, wo_hbm, wv_hbm, wp_hbm, wg_hbm, wu_hbm, wd_hbm,
     mixer_out, expert_out,
     wi, wo, wv, wp, wg, wu, wd,
-    tok_send, tok, mrows, send, rows, hid, res, ret, gat, ext, ogate, acc, rim_s, rim_r, slot_rows, cols,
-    load_sem, tok_ss, tok_rs, mix_ss, mix_rs, disp_ss, disp_rs, row_ss, row_rs, hid_ss, hid_rs,
+    tok, mrows, send, near, rows, hid, res, ret, gat, ext, ogate, acc, rim_s, rim_r, slot_rows, cols,
+    load_sem, tok_ss, tok_rs, mix_ss, mix_rs, disp_ss, near_ss, disp_rs, row_ss, row_rs, hid_ss, hid_rs,
     ret_ss, ret_rs, gat_ss, gat_rs, rim_ss, rim_rs,
 ):
     ep, tp = lax.axis_index("ep"), lax.axis_index("tp")
@@ -70,16 +74,16 @@
 
     normed = rms_rows(expert_in[...], expert_gain[...])
     for k in range(X):
-        tok_send[k] = normed[:, k * 512 : (k + 1) * 512]
+        tok[tp, k] = normed[:, k * 512 : (k + 1) * 512]
     mrows[tp] = rms_rows(mixer_in[...], mixer_gain[...])
-    tok[tp] = tok_send[tp]
 
     pl.semaphore_wait(barrier, EP + 2)
 
-    for i, other in enumerate((right, left, far)):
-        to_tp(tok_send.at[other], tok.at[tp], tok_ss, tok_rs, other).start()
-    to_tp(mrows.at[tp], mrows.at[tp], mix_ss.at[0], mix_rs.at[0], right).start()
-    to_tp(mrows.at[tp], mrows.at[tp], mix_ss.at[1], mix_rs.at[1], left).start()
+    for i in range(X):
+        k = lax.rem(tp + 1 + i, X)
+        to_tp(tok.at[tp, k], tok.at[tp, k], tok_ss.at[0], tok_rs.at[0, i], right).start()
+        k = lax.rem(tp + 2 * X - 1 - i, X)
+        to_tp(tok.at[tp, k], tok.at[tp, k], tok_ss.at[1], tok_rs.at[1, i], left).start()
 
     count = ids.shape[1]
     labels = lax.broadcasted_iota(jnp.int32, (EP, count), 0)
@@ -97,16 +101,28 @@
         cols[k] = jnp.transpose(jnp.broadcast_to(slot, (128, count)))
         cols[2 + k] = jnp.transpose(jnp.broadcast_to(weights[k : k + 1, :] / total, (128, count)))
 
-    await_recv(tok.at[pl.ds(0, 3)], tok_rs)
-
-    @pl.loop(0, Z)
+    def token_pass(side, i, other, source):
+        k = lax.rem(tp + i, X) if side == 0 else lax.rem(tp + X - i, X)
+        await_recv(tok.at[source, k], tok_rs.at[side, i])
+        if i in ((1, 2) if side == 0 else (2, 3)):
+            piece = tok.at[source, k]
+            to_tp(piece, piece, tok_ss.at[2], tok_rs.at[2 + side, i], other).start()
+
+    token_pass(0, 0, right, left)
+    token_pass(0, 1, right, left)
+    token_pass(1, 0, left, right)
+    to_tp(mrows.at[tp], mrows.at[tp], mix_ss.at[0], mix_rs.at[0], right).start()
+    to_tp(mrows.at[tp], mrows.at[tp], mix_ss.at[1], mix_rs.at[1], left).start()
+    await_recv(tok.at[far, tp], tok_rs.at[2, 1])
+
+    @pl.loop(0, FAR)
     def _(step):
         plane = lax.rem(z + offset_of(step), Z)
         index = (lax.broadcasted_iota(jnp.int32, (PLANE * CAP, count), 0) + plane * (PLANE * CAP)).astype(jnp.float32)
         pick = (index == slot_rows[0:1, :]) | (index == slot_rows[1:2, :])
         moved = jnp.dot(
             jnp.where(pick, 1.0, 0.0).astype(jnp.bfloat16),
-            tok[...].reshape(count, 512),
+            tok[:, tp].reshape(count, 512),
             preferred_element_type=jnp.float32,
         )
         send[pl.ds(plane * PLANE, PLANE)] = moved.reshape(PLANE, CAP, 512).astype(jnp.bfloat16)
@@ -115,13 +131,12 @@
         def _(j):
             target = plane * PLANE + j
 
-            @pl.when(target != ep)
-            def _():
-                to_ep(send.at[target], rows.at[tp, ep], disp_ss, disp_rs.at[step], target).start()
-
-            @pl.when(target == ep)
-            def _():
-                rows[tp, ep] = send[ep]
+            to_ep(send.at[target], rows.at[tp, ep], disp_ss, disp_rs.at[step], target).start()
+
+    token_pass(0, 2, right, left)
+    token_pass(0, 3, right, left)
+    for i in range(1, X):
+        token_pass(1, i, left, right)
 
     half = mrows.shape[1] // 2
     await_recv(mrows.at[left], mix_rs.at[0])
@@ -131,6 +146,34 @@
     piece = mrows.at[right, pl.ds(half, half)]
     to_tp(piece, piece, mix_ss.at[2], mix_rs.at[3], left).start()
 
+    await_recv(tok.at[far, lax.rem(tp + 1, X)], tok_rs.at[2, 2])
+    await_recv(tok.at[far, lax.rem(tp + 3, X)], tok_rs.at[3, 2])
+    await_recv(tok.at[far, lax.rem(tp + 2, X)], tok_rs.at[3, 3])
+
+    @pl.loop(FAR, Z)
+    def _(step):
+        plane = lax.rem(z + offset_of(step), Z)
+        index = (lax.broadcasted_iota(jnp.int32, (PLANE * CAP, count), 0) + plane * (PLANE * CAP)).astype(jnp.float32)
+        pick = (index == slot_rows[0:1, :]) | (index == slot_rows[1:2, :])
+        pick = jnp.where(pick, 1.0, 0.0).astype(jnp.bfloat16)
+        first = (step - FAR) * PLANE
+        for k in range(X):
+            moved = jnp.dot(pick, tok[:, k].reshape(count, 512), preferred_element_type=jnp.float32)
+            near[pl.ds(first, PLANE), k] = moved.reshape(PLANE, CAP, 512).astype(jnp.bfloat16)
+
+        @pl.loop(0, PLANE)
+        def _(j):
+            target = plane * PLANE + j
+
+            @pl.when(target != ep)
+            def _():
+                to_ep(near.at[first + j], rows.at[:, ep], near_ss, disp_rs.at[step], target).start()
+
+            @pl.when(target == ep)
+            def _():
+                for k in range(X):
+                    rows[k, ep] = near[first + j, k]
+
     def ring_send(buf, ss, rs, plane, step):
         block = buf.at[tp, pl.ds(plane * PLANE, PLANE)]
         to_tp(block, block, ss.at[0], rs.at[0, step], right).start()
@@ -162,12 +205,24 @@
 
     def stage_rows(step):
         plane = source_plane(step)
-        await_plane(rows.at[tp], plane, disp_rs, step)
+        await_recv(rows.at[tp, pl.ds(plane * PLANE, PLANE)], disp_rs.at[step])
         ring_send(rows, row_ss, row_rs, plane, step)
 
     def stage_gate_up(step):
         plane = source_plane(step)
-        ring_end(rows, row_rs, plane, step)
+
+        @pl.when(step < FAR)
+        def _():
+            ring_end(rows, row_rs, plane, step)
+
+        @pl.when((step >= FAR) & (step < Z - 1))
+        def _():
+            await_recv(rows.at[:, pl.ds(plane * PLANE, PLANE)], disp_rs.at[step])
+
+        @pl.when(step == Z - 1)
+        def _():
+            await_recv(rows.at[:, pl.ds(plane * PLANE, PLANE - 1)], disp_rs.at[step])
+
         gate = up = None
         for k in range(X):
             x = rows[k, pl.ds(plane * PLANE, PLANE)].reshape(PLANE * CAP, 512)
@@ -254,11 +309,11 @@
 
     @pl.loop(2, Z + 5)
     def _(s):
-        @pl.when(s < Z)
+        @pl.when(s < FAR)
         def _():
             stage_rows(s)
 
-        @pl.when(s < Z + 2)
+        @pl.when(s < FAR + 2)
         def _():
             ring_pass(rows, row_ss, row_rs, source_plane(s - 2), s - 2)
 
@@ -283,9 +338,9 @@
             to_tp(gat.at[tp], gat.at[tp], gat_ss.at[0], gat_rs.at[0], right).start()
             to_tp(gat.at[tp], gat.at[tp], gat_ss.at[1], gat_rs.at[1], left).start()
 
-        @pl.when(s >= 7)
-        def _():
-            stage_combine(s - 7)
+        @pl.when(s >= LAG)
+        def _():
+            stage_combine(s - LAG)
 
     half_g = count // 2
     await_recv(gat.at[left], gat_rs.at[0])
@@ -294,8 +349,11 @@
     await_recv(gat.at[right], gat_rs.at[1])
     piece = gat.at[right, pl.ds(half_g, half_g)]
     to_tp(piece, piece, gat_ss.at[2], gat_rs.at[3], left).start()
-    stage_combine(Z - 2)
-    stage_combine(Z - 1)
+
+    @pl.loop(Z + 5 - LAG, Z)
+    def _(step):
+        stage_combine(step)
+
     expert_out[...] = acc[...].astype(jnp.bfloat16)
     await_recv(gat.at[far, pl.ds(0, half_g)], gat_rs.at[2])
     await_recv(gat.at[far, pl.ds(half_g, half_g)], gat_rs.at[3])
@@ -309,13 +367,27 @@
             out = o if k == 0 else out + o
         mixer_out[:, span] = out.astype(jnp.bfloat16)
 
-    await_send(tok.at[pl.ds(0, 3)], tok_ss)
-    await_send(send.at[pl.ds(0, EP - 1)], disp_ss)
+    await_send(send.at[pl.ds(0, FAR * PLANE)], disp_ss)
+    await_send(near.at[pl.ds(0, (Z - FAR) * PLANE - 1)], near_ss)
     await_send(res.at[pl.ds(0, EP - 1)], ret_ss)
     await_send(rim_s, rim_ss)
-    for buf, sem in ((mrows, mix_ss), (rows, row_ss), (hid, hid_ss), (gat, gat_ss)):
+    for buf, sem in ((tok, tok_ss), (mrows, mix_ss), (hid, hid_ss), (gat, gat_ss)):
         for i in range(3):
             await_send(buf.at[0], sem.at[i])
+    for i in range(3):
+        await_send(rows.at[0, pl.ds(0, FAR * PLANE)], row_ss.at[i])
+
+
+def hand_over(mixer_in, expert_in, mixer_out, expert_out, held, in_sem, out_sem):
+    ins = [pltpu.make_async_copy(src, held.at[i], in_sem.at[i]) for i, src in enumerate((mixer_in, expert_in))]
+    outs = [pltpu.make_async_copy(held.at[i], dst, out_sem.at[i]) for i, dst in enumerate((mixer_out, expert_out))]
+    for copy in ins:
+        copy.start()
+    for i in range(2):
+        ins[i].wait()
+        outs[i].start()
+    for copy in outs:
+        copy.wait()
 
 
 def on_device(
@@ -329,19 +401,19 @@
     remote = pl.BlockSpec(memory_space=pl.ANY)
     dma, vmem = pltpu.SemaphoreType.DMA, pltpu.VMEM
     out = jax.ShapeDtypeStruct((count, 512), bf16)
-    return pl.pallas_call(
+    results = pl.pallas_call(
         kernel,
         out_shape=(out, out),
         in_specs=[local] * 7 + [remote] * 7,
         out_specs=(local, local),
         scratch_shapes=[
             *[vmem((wide, 512), bf16)] * 4, *[vmem((wide, 256), bf16)] * 2, vmem((1024, 512), bf16),
-            vmem((X, own, 512), bf16), vmem((X, own, 512), bf16), vmem((X, own, wide), bf16),
-            vmem((EP, CAP, 512), bf16), vmem((X, EP, CAP, 512), bf16), vmem((X, EP, CAP, 256), bf16),
+            vmem((X, X, own, 512), bf16), vmem((X, own, wide), bf16),
+            vmem((EP, CAP, 512), bf16), vmem(((Z - FAR) * PLANE, X, CAP, 512), bf16), vmem((X, EP, CAP, 512), bf16), vmem((X, EP, CAP, 256), bf16),
             vmem((EP, CAP, 512), bf16), vmem((EP, CAP, 512), bf16), vmem((X, count, 512), bf16),
             vmem((count + 8, 512), f32), vmem((count, 512), f32), vmem((count, 512), f32),
             vmem((16, 512), bf16), vmem((16, 512), bf16), vmem((8, count), f32), vmem((4, count, 128), f32),
-            dma((7,)), dma, dma, dma((3,)), dma((4,)), dma, dma((Z,)), dma((3,)), dma((4, Z)), dma((3,)), dma((4, Z)),
+            dma((7,)), dma((3,)), dma((4, X)), dma((3,)), dma((4,)), dma, dma, dma((Z,)), dma((3,)), dma((4, Z)), dma((3,)), dma((4, Z)),
             dma, dma((Z,)), dma((3,)), dma((4,)), dma, dma,
         ],
         compiler_params=pltpu.CompilerParams(
@@ -353,6 +425,14 @@
         route_ids.T, route_weights.T,
         in_gate_weight, out_gate_weight, value_weight, mixer_proj, gate_weight[0], up_weight[0], down_weight[0],
     )
+    return pl.pallas_call(
+        hand_over,
+        out_shape=(out, out),
+        in_specs=[remote] * 2,
+        out_specs=(remote, remote),
+        scratch_shapes=[vmem((2, count, 512), bf16), dma((2,)), dma((2,))],
+        name="hand_over",
+    )(*results)
 
 
 def solution(mesh):

time: 138 us -> 133 us (0.964)
  the two profiles are of different devices: /device:TPU:25 before, /device:TPU:1 now
where the time goes in v2:
time: 133 us; the launch traced here: 130 us
  Pallas kernels  129 us (97%)
    pallas_call x1, Pallas kernels, on_device(): pl.pallas_call(kernel, out_shape=(out, out), in_specs=[local] * 7 + [remo...  128 us

profile of v2, /device:TPU:1, one launch (start us, length us, event | category | flops | bytes accessed | tf_op | source)
XLA Modules:
  0.0 130.1 jit_solution(5561812047684768623)
XLA Ops:
  0.6 127.5 %mixer_and_experts.1 = (bf16[384,512]{1,0:T(8,128)(2,1)}, bf16[384,512]{1,0:T(8,128)(2,1)}) custom-call(bf16[96,2048]{1,0:T(8,128)(2,1)} %mixer_in.1, bf16[96,2048]{1,0:T(8,128)(2,1)} %expert_in.1, f32[1,2048]{1,0:T(1,128)} %bitcast.10, f32[1,2048]{1,0:T(1,128)} %bitcast.11, f32[3,2048]{1,0:T(4,128)} %taps.1, s32[2,384]{1,0:T(2,128)} %bitcast.12, ...), custom_call_target="tpu_custom_call" | custom-call | tf_op jit(solution)/shard_map/mixer_and_experts/pallas_call | solution.py:404
  128.1 1.9 %hand_over.1 = (bf16[384,512]{1,0:T(8,128)(2,1)}, bf16[384,512]{1,0:T(8,128)(2,1)}) custom-call(bf16[384,512]{1,0:T(8,128)(2,1)} %get-tuple-element.4.mixer_in, bf16[384,512]{1,0:T(8,128)(2,1)} %get-tuple-element.5.expert_in), custom_call_target="tpu_custom_call" | custom-call | tf_op jit(solution)/shard_map/hand_over/pallas_call | solution.py:428

commit v3 on v1

v3 whole, which is shorter than its diff:
```python
import jax
import jax.numpy as jnp
from jax import lax
from jax.experimental import pallas as pl
from jax.experimental.pallas import tpu as pltpu
from jax.sharding import PartitionSpec as P

norm_eps = 1e-06
Z, Y, C, X = 8, 4, 2, 4
PLANE = Y * C
EP = Z * PLANE
CHIPS = Z * Y
CAP = 24
SEND = (0, 1, 7, 2, 6, 3, 5, 4)
BACK = (4, 3, 5, 2, 6, 1, 7, 0)
PAIR, DOWN = 6, 8
MESH = pl.DeviceIdType.MESH


def pick_of(table, step):
    value = table[0]
    for at in range(1, len(table)):
        value = jnp.where(step == at, table[at], value)
    return value


def rms_rows(values, gain_row):
    wide = values.astype(jnp.float32)
    scale = lax.rsqrt(jnp.mean(wide * wide, axis=-1, keepdims=True) + norm_eps)
    return (wide * scale * gain_row).astype(jnp.bfloat16)


def kernel(
    mixer_in, expert_in, mixer_gain, expert_gain, taps, ids, weights,
    wi_hbm, wo_hbm, wv_hbm, wp_hbm, wg_hbm, wu_hbm, wd_hbm,
    mixer_out, expert_out,
    wi, wo, wv, wp, wg, wu, wd,
    route, tok_send, tok, mrows, send, rows, hid, res, ret, gat, ext, ogate, acc, rim_s, rim_r, slot_rows, cols,
    fin, fin_same, fin_pair,
    load_sem, wt_ss, wt_rs, route_ss, route_rs, tok_ss, tok_rs, mix_ss, mix_rs, disp_ss, disp_rs, row_ss, row_rs,
    hid_ss, hid_rs, ret_ss, ret_rs, gat_ss, gat_rs, rim_ss, rim_rs, fin_ss, fin_rs,
):
    ep, tp = lax.axis_index("ep"), lax.axis_index("tp")
    z, core = ep // PLANE, lax.rem(ep, C)
    chip, twin = ep // C, ep + 1 - 2 * core
    odd = lax.rem(tp, 2)
    pair = tp + 1 - 2 * odd
    mate = lax.rem(tp + 3 + 2 * odd, X)
    far = lax.rem(tp + 2, X)
    u = 1 - odd
    first = lax.rem(tp + X - u, X)
    count = ids.shape[1]

    loads = [
        pltpu.make_async_copy(src, dst, load_sem.at[i])
        for i, (src, dst) in enumerate(
            ((wg_hbm, wg.at[0]), (wu_hbm, wu.at[0]), (wd_hbm, wd.at[0]),
             (wi_hbm, wi), (wo_hbm, wo), (wv_hbm, wv), (wp_hbm, wp))
        )
    ]
    for load in loads:
        load.start()

    barrier = pltpu.get_barrier_semaphore()

    @pl.loop(1, EP)
    def _(d):
        pl.semaphore_signal(barrier, inc=1, device_id={"ep": lax.rem(ep + d, EP)}, device_id_type=MESH)

    for other in (pair, mate):
        pl.semaphore_signal(barrier, inc=1, device_id={"tp": other}, device_id_type=MESH)
        pl.semaphore_signal(barrier, inc=1, device_id={"ep": twin, "tp": other}, device_id_type=MESH)

    def to_ep(src, dst, ss, rs, target):
        return pltpu.make_async_remote_copy(src, dst, ss, rs, device_id={"ep": target}, device_id_type=MESH)

    def to_tp(src, dst, ss, rs, target):
        return pltpu.make_async_remote_copy(src, dst, ss, rs, device_id={"tp": target}, device_id_type=MESH)

    def to_twin(src, dst, ss, rs, target):
        return pltpu.make_async_remote_copy(
            src, dst, ss, rs, device_id={"ep": twin, "tp": target}, device_id_type=MESH
        )

    def await_recv(ref, sem):
        to_tp(ref, ref, sem, sem, mate).wait_recv()

    def await_send(ref, sem):
        to_tp(ref, ref, sem, sem, mate).wait_send()

    picks = jnp.concatenate(
        [ids[...].astype(jnp.float32), weights[...], jnp.zeros((4, count), jnp.float32)], axis=0
    )
    turned = jnp.where((first == 1) == (core == 0), pltpu.roll(picks, 3 * count // 4, 1), pltpu.roll(picks, count // 4, 1))
    route[core] = turned
    normed = rms_rows(expert_in[...], expert_gain[...])
    for k in range(X):
        tok_send[k] = normed[:, k * 512 : (k + 1) * 512]
    tok[core, u] = tok_send[2 * u + core]
    mrows[tp] = rms_rows(mixer_in[...], mixer_gain[...])

    for load in loads[:3]:
        load.wait()
    pl.semaphore_wait(barrier, EP + 3)

    to_ep(route.at[core], route.at[core], route_ss, route_rs, twin).start()
    to_twin(tok_send.at[2 * (1 - u) + 1 - core], tok.at[core, u], tok_ss, tok_rs, mate).start()
    to_tp(tok_send.at[2 * (1 - u) + core], tok.at[core, u], tok_ss, tok_rs, mate).start()
    to_ep(tok_send.at[2 * u + 1 - core], tok.at[core, u], tok_ss, tok_rs, twin).start()
    to_tp(wg.at[0], wg.at[1], wt_ss.at[0], wt_rs.at[0], pair).start()
    to_tp(wu.at[0], wu.at[1], wt_ss.at[1], wt_rs.at[1], pair).start()
    to_tp(mrows.at[tp], mrows.at[tp], mix_ss.at[0], mix_rs.at[0], pair).start()
    to_tp(wd.at[0], wd.at[1], wt_ss.at[2], wt_rs.at[2], pair).start()

    await_recv(route.at[1 - core], route_rs)
    lane = lax.broadcasted_iota(jnp.int32, (8, count), 1)
    both = jnp.where(lane < count // 2, route[0], route[1])
    labels = lax.broadcasted_iota(jnp.int32, (EP, count), 0).astype(jnp.float32)
    hot = [both[k : k + 1, :] == labels for k in range(2)]
    named = jnp.where(hot[0] | hot[1], 1.0, 0.0).astype(jnp.bfloat16)
    older = (
        lax.broadcasted_iota(jnp.int32, (count, count), 0) < lax.broadcasted_iota(jnp.int32, (count, count), 1)
    )
    earlier = jnp.dot(named, jnp.where(older, 1.0, 0.0).astype(jnp.bfloat16), preferred_element_type=jnp.float32)
    total = both[2:3, :] + both[3:4, :]
    for k in range(2):
        within = jnp.sum(jnp.where(hot[k], earlier, 0.0), axis=0, keepdims=True)
        slot = both[k : k + 1, :] * CAP + within
        slot_rows[k : k + 1, :] = slot
        cols[k] = jnp.transpose(jnp.broadcast_to(slot, (128, count)))
        cols[2 + k] = jnp.transpose(jnp.broadcast_to(both[2 + k : 3 + k, :] / total, (128, count)))

    await_recv(send.at[pl.ds(0, 12)], tok_rs)
    to_tp(mrows.at[tp], mrows.at[tp], mix_ss.at[1], mix_rs.at[1], mate).start()

    @pl.loop(0, Z)
    def _(step):
        plane = lax.rem(z + pick_of(SEND, step), Z)
        index = (lax.broadcasted_iota(jnp.int32, (PLANE * CAP, count), 0) + plane * (PLANE * CAP)).astype(jnp.float32)
        pick = (index == slot_rows[0:1, :]) | (index == slot_rows[1:2, :])
        moved = jnp.dot(
            jnp.where(pick, 1.0, 0.0).astype(jnp.bfloat16),
            tok[...].reshape(count, 512),
            preferred_element_type=jnp.float32,
        )
        send[pl.ds(plane * PLANE, PLANE)] = moved.reshape(PLANE, CAP, 512).astype(jnp.bfloat16)

        @pl.loop(0, PLANE)
        def _(j):
            target = plane * PLANE + j

            @pl.when(target != ep)
            def _():
                to_ep(send.at[target], rows.at[2 * u + core, chip], disp_ss, disp_rs.at[step], target).start()

            @pl.when(target == ep)
            def _():
                rows[2 * u + core, chip] = send[ep]

    def source_chips(offset):
        return pl.ds(lax.rem(z + Z - offset, Z) * Y, Y)

    def await_slabs(sem, last):
        @pl.when(last)
        def _():
            await_recv(send.at[pl.ds(0, PLANE - 1)], sem)

        @pl.when(jnp.logical_not(last))
        def _():
            await_recv(send.at[pl.ds(0, PLANE)], sem)

    def stage_rows(step):
        block = rows.at[pl.ds(2 * u, 2), source_chips(pick_of(SEND, step))]
        await_slabs(disp_rs.at[step], step == SEND.index(0))
        to_tp(block, block, row_ss, row_rs.at[step], mate).start()

    def stage_gate_up(chips, which, sem):
        gate = up = None
        for k in range(X):
            x = rows[k, chips].reshape(Y * CAP, 512)
            g = jnp.dot(x, wg[which, k * 512 : (k + 1) * 512, :], preferred_element_type=jnp.float32)
            v = jnp.dot(x, wu[which, k * 512 : (k + 1) * 512, :], preferred_element_type=jnp.float32)
            gate, up = (g, v) if k == 0 else (gate + g, up + v)
        h = gate / (1.0 + jnp.exp(-gate)) * up
        place = (tp, pair)[which]
        hid[place, chips] = h.reshape(Y, CAP, 256).astype(jnp.bfloat16)
        to_tp(hid.at[place, chips], hid.at[place, chips], hid_ss, sem, mate).start()

    def stage_down(step, which):
        offset = pick_of((SEND, BACK)[which], step)
        chips = source_chips(offset)
        out = None
        for k in range(X):
            h = hid[k, chips].reshape(Y * CAP, 256)
            o = jnp.dot(h, wd[which, k * 256 : (k + 1) * 256, :], preferred_element_type=jnp.float32)
            out = o if k == 0 else out + o
        res[which, chips] = out.reshape(Y, CAP, 512).astype(jnp.bfloat16)

        @pl.loop(0, Y)
        def _(j):
            goal = lax.rem(z + Z - offset, Z) * Y + j
            target = goal * C + which

            @pl.when(target != ep)
            def _():
                to_ep(res.at[which, goal], ret.at[ep], ret_ss.at[which], ret_rs.at[step], target).start()

            @pl.when(target == ep)
            def _():
                ret[ep] = res[which, goal]

    def stage_combine(step):
        offset = jnp.where(core == 0, pick_of(SEND, step), pick_of(BACK, step))
        plane = lax.rem(z + offset, Z)
        await_slabs(ret_rs.at[step], offset == 0)
        index = lax.broadcasted_iota(jnp.int32, (count, PLANE * CAP), 1) + plane * (PLANE * CAP)
        index = index.astype(jnp.float32)
        share = jnp.where(cols[0][:, 0:1] == index, cols[2][:, 0:1], 0.0)
        share = jnp.where(cols[1][:, 0:1] == index, cols[3][:, 0:1], share)
        high = share.astype(jnp.bfloat16)
        low = (share - high.astype(jnp.float32)).astype(jnp.bfloat16)
        got = ret[pl.ds(plane * PLANE, PLANE)].reshape(PLANE * CAP, 512)
        acc[...] += jnp.dot(high, got, preferred_element_type=jnp.float32) + jnp.dot(
            low, got, preferred_element_type=jnp.float32
        )

    acc[...] = jnp.zeros(acc.shape, jnp.float32)

    def stage_own(step):
        chips = source_chips(pick_of(SEND, step))
        await_recv(rows.at[pl.ds(2 * (1 - u), 2), chips], row_rs.at[step])
        stage_gate_up(chips, 0, hid_rs.at[0, step])

    def stage_pair(step):
        stage_gate_up(source_chips(pick_of(SEND, step)), 1, hid_rs.at[1, step])

    def stage_down_own(step):
        chips = source_chips(pick_of(SEND, step))
        await_recv(hid.at[mate, chips], hid_rs.at[0, step])
        await_recv(hid.at[far, chips], hid_rs.at[1, step])
        stage_down(step, 0)

    @pl.loop(0, DOWN + Z // 2)
    def _(s):
        @pl.when(s < Z)
        def _():
            stage_rows(s)

        @pl.when((s >= 1) & (s < Z + 1))
        def _():
            stage_own(s - 1)

        @pl.when(s == PAIR)
        def _():
            await_recv(wg.at[1], wt_rs.at[0])
            await_recv(wu.at[1], wt_rs.at[1])

        @pl.when((s >= PAIR) & (s < PAIR + Z // 2))
        def _():
            stage_pair(2 * (s - PAIR))
            stage_pair(2 * (s - PAIR) + 1)

        @pl.when(s == PAIR + Z // 2)
        def _():
            await_recv(mrows.at[pair], mix_rs.at[0])
            to_tp(mrows.at[pair], mrows.at[pair], mix_ss.at[2], mix_rs.at[2], mate).start()

        @pl.when(s >= DOWN)
        def _():
            stage_down_own(2 * (s - DOWN))
            stage_down_own(2 * (s - DOWN) + 1)

    await_recv(mrows.at[mate], mix_rs.at[1])
    for load in loads[3:]:
        load.wait()
    await_recv(mrows.at[far], mix_rs.at[2])

    @pl.loop(0, 2)
    def _(n):
        span = pl.ds(pl.multiple_of(n * 256, 256), 256)
        m = mrows[...].reshape(count, 2048)
        in_gate = jnp.dot(m, wi[:, span], preferred_element_type=jnp.float32)
        values = jnp.dot(m, wv[:, span], preferred_element_type=jnp.float32)
        product = (in_gate * values).astype(jnp.bfloat16)
        ext[8:, span] = product.astype(jnp.float32)
        rim_s[:, span] = product[count - 16 :]
        ogate[:, span] = jnp.dot(m, wo[:, span], preferred_element_type=jnp.float32)

    to_ep(rim_s, rim_r, rim_ss, rim_rs, lax.rem(ep + 1, EP)).start()

    await_recv(wd.at[1], wt_rs.at[2])

    @pl.loop(0, Z)
    def _(s):
        stage_down(s, 1)

    await_recv(rim_r, rim_rs)
    before = rim_r[...].astype(jnp.float32)[8:]
    ext[0:8, :] = jnp.where(ep == 0, jnp.zeros_like(before), before)

    @pl.loop(0, 4)
    def _(n):
        span = pl.ds(pl.multiple_of(n * 128, 128), 128)
        tap_span = pl.ds(pl.multiple_of(tp * 512 + n * 128, 128), 128)
        conv = taps[0:1, tap_span] * ext[6 : 6 + count, span]
        conv = conv + taps[1:2, tap_span] * ext[7 : 7 + count, span]
        conv = conv + taps[2:3, tap_span] * ext[8 : 8 + count, span]
        gat[tp, :, span] = (ogate[:, span] * conv).astype(jnp.bfloat16)

    to_tp(gat.at[tp], gat.at[tp], gat_ss.at[0], gat_rs.at[0], pair).start()
    to_tp(gat.at[tp], gat.at[tp], gat_ss.at[1], gat_rs.at[1], mate).start()

    @pl.loop(0, Z - 3)
    def _(s):
        stage_combine(s)

    await_recv(gat.at[pair], gat_rs.at[0])
    to_tp(gat.at[pair], gat.at[pair], gat_ss.at[2], gat_rs.at[2], mate).start()

    @pl.loop(Z - 3, Z)
    def _(s):
        stage_combine(s)

    fin[...] = acc[...].astype(jnp.bfloat16).reshape(C, count // 2, 512)

    @pl.when(core == 0)
    def _():
        to_ep(fin.at[1], fin_same, fin_ss.at[0], fin_rs.at[0], twin).start()

    @pl.when(core == 1)
    def _():
        to_tp(fin.at[1], fin_pair, fin_ss.at[0], fin_rs.at[1], pair).start()
        to_twin(fin.at[0], fin_pair, fin_ss.at[1], fin_rs.at[1], pair).start()

    await_recv(gat.at[mate], gat_rs.at[1])
    await_recv(gat.at[far], gat_rs.at[2])

    @pl.loop(0, 2)
    def _(n):
        span = pl.ds(pl.multiple_of(n * 256, 256), 256)
        out = None
        for k in range(X):
            o = jnp.dot(gat[k], wp[k * 512 : (k + 1) * 512, span], preferred_element_type=jnp.float32)
            out = o if k == 0 else out + o
        mixer_out[:, span] = out.astype(jnp.bfloat16)

    own = count // 4

    @pl.when(core == 0)
    def _():
        expert_out[first] = fin[0, 0:own]
        expert_out[lax.rem(first + 1, X)] = fin[0, own:]
        await_send(fin.at[1], fin_ss.at[0])

    @pl.when(core == 1)
    def _():
        await_recv(fin_same, fin_rs.at[0])
        expert_out[first] = fin_same[0:own]
        expert_out[lax.rem(first + 1, X)] = fin_same[own:]
        await_send(fin.at[1], fin_ss.at[0])
        await_send(fin.at[0], fin_ss.at[1])

    await_recv(fin_pair, fin_rs.at[1])
    expert_out[lax.rem(first + 2, X)] = fin_pair[0:own]
    expert_out[lax.rem(first + 3, X)] = fin_pair[own:]

    await_send(route.at[0], route_ss)
    await_send(send.at[pl.ds(0, 12)], tok_ss)
    await_send(rim_s, rim_ss)
    for buf, sem in ((wg.at[0], wt_ss.at[0]), (wu.at[0], wt_ss.at[1]), (wd.at[0], wt_ss.at[2])):
        await_send(buf, sem)
    for i in range(3):
        await_send(mrows.at[0], mix_ss.at[i])
        await_send(gat.at[0], gat_ss.at[i])
    await_send(send.at[pl.ds(0, EP - 1)], disp_ss)
    await_send(rows.at[pl.ds(0, 2)], row_ss)
    await_send(hid.at[pl.ds(0, 2)], hid_ss)
    for which in range(C):

        @pl.when(core == which)
        def _():
            await_send(ret.at[pl.ds(0, CHIPS - 1)], ret_ss.at[which])

        @pl.when(core != which)
        def _():
            await_send(ret.at[pl.ds(0, CHIPS)], ret_ss.at[which])


def hand_over(mixer_in, expert_in, mixer_out, expert_out, held, in_sem, out_sem):
    ins = [pltpu.make_async_copy(src, held.at[i], in_sem.at[i]) for i, src in enumerate((mixer_in, expert_in))]
    outs = [pltpu.make_async_copy(held.at[i], dst, out_sem.at[i]) for i, dst in enumerate((mixer_out, expert_out))]
    for copy in ins:
        copy.start()
    for i in range(2):
        ins[i].wait()
        outs[i].start()
    for copy in outs:
        copy.wait()


def on_device(
    mixer_in, expert_in, mixer_gain, in_gate_weight, out_gate_weight, value_weight, conv_taps, mixer_proj,
    expert_gain, route_ids, route_weights, gate_weight, up_weight, down_weight,
):
    bf16, f32 = jnp.bfloat16, jnp.float32
    own, wide = mixer_in.shape
    count = route_ids.shape[0]
    local = pl.BlockSpec(memory_space=pltpu.VMEM)
    remote = pl.BlockSpec(memory_space=pl.ANY)
    dma, vmem = pltpu.SemaphoreType.DMA, pltpu.VMEM
    out = jax.ShapeDtypeStruct((count, 512), bf16)
    results = pl.pallas_call(
        kernel,
        out_shape=(out, jax.ShapeDtypeStruct((X, own, 512), bf16)),
        in_specs=[local] * 7 + [remote] * 7,
        out_specs=(local, local),
        scratch_shapes=[
            *[vmem((wide, 512), bf16)] * 4, *[vmem((2, wide, 256), bf16)] * 2, vmem((2, 1024, 512), bf16),
            vmem((C, 8, count), f32), vmem((X, own, 512), bf16), vmem((C, 2, own, 512), bf16), vmem((X, own, wide), bf16),
            vmem((EP, CAP, 512), bf16), vmem((X, CHIPS, CAP, 512), bf16), vmem((X, CHIPS, CAP, 256), bf16),
            vmem((C, CHIPS, CAP, 512), bf16), vmem((EP, CAP, 512), bf16), vmem((X, count, 512), bf16),
            vmem((count + 8, 512), f32), vmem((count, 512), f32), vmem((count, 512), f32),
            vmem((16, 512), bf16), vmem((16, 512), bf16), vmem((8, count), f32), vmem((4, count, 128), f32),
            vmem((C, count // 2, 512), bf16), vmem((count // 2, 512), bf16), vmem((count // 2, 512), bf16),
            dma((7,)), dma((3,)), dma((3,)), dma, dma, dma, dma, dma((3,)), dma((3,)), dma, dma((Z,)), dma, dma((Z,)),
            dma, dma((2, Z)), dma((2,)), dma((Z,)), dma((3,)), dma((3,)), dma, dma, dma((2,)), dma((2,)),
        ],
        compiler_params=pltpu.CompilerParams(
            collective_id=0, has_side_effects=True, vmem_limit_bytes=62 * 2**20
        ),
        name="mixer_and_experts",
    )(
        mixer_in, expert_in, mixer_gain.reshape(1, -1), expert_gain.reshape(1, -1), conv_taps,
        route_ids.T, route_weights.T,
        in_gate_weight, out_gate_weight, value_weight, mixer_proj, gate_weight[0], up_weight[0], down_weight[0],
    )
    return pl.pallas_call(
        hand_over,
        out_shape=(out, out),
        in_specs=[remote] * 2,
        out_specs=(remote, remote),
        scratch_shapes=[vmem((2, count, 512), bf16), dma((2,)), dma((2,))],
        name="hand_over",
    )(results[0], results[1].reshape(count, 512))


def solution(mesh):
    return jax.shard_map(
        on_device,
        mesh=mesh,
        in_specs=(
            P(("ep", "tp"), None),
            P(("ep", "tp"), None),
            P(),
            P(None, "tp"),
            P(None, "tp"),
            P(None, "tp"),
            P(),
            P(None, "tp"),
            P(),
            P("ep", None),
            P("ep", None),
            P("ep", None, "tp"),
            P("ep", None, "tp"),
            P("ep", None, "tp"),
        ),
        out_specs=(P("ep", "tp"), P("ep", "tp")),
        check_vma=False,
    )
```

time: 138 us -> 126 us (0.913)
  the two profiles are of different devices: /device:TPU:25 before, /device:TPU:1 now
where the time goes in v3:
time: 126 us; the launch traced here: 125 us
  Pallas kernels  125 us (99%)
    pallas_call x1, Pallas kernels, on_device(): pl.pallas_call(kernel, out_shape=(out, jax.ShapeDtypeStruct((X, own, 512)...  123 us

profile of v3, /device:TPU:1, one launch (start us, length us, event | category | flops | bytes accessed | tf_op | source)
XLA Modules:
  0.0 125.4 jit_solution(4646788721242802821)
XLA Ops:
  0.6 122.9 %mixer_and_experts.1 = (bf16[384,512]{1,0:T(8,128)(2,1)}, bf16[4,96,512]{2,1,0:T(8,128)(2,1)}) custom-call(bf16[96,2048]{1,0:T(8,128)(2,1)} %mixer_in.1, bf16[96,2048]{1,0:T(8,128)(2,1)} %expert_in.1, f32[1,2048]{1,0:T(1,128)} %bitcast.12, f32[1,2048]{1,0:T(1,128)} %bitcast.13, f32[3,2048]{1,0:T(4,128)} %taps.1, s32[2,384]{1,0:T(2,128)} %bitcast.14, ...), custom_call_target="tpu_custom_call" | custom-call | tf_op jit(solution)/shard_map/mixer_and_experts/pallas_call | solution.py:412
  123.5 1.9 %hand_over.1 = (bf16[384,512]{1,0:T(8,128)(2,1)}, bf16[384,512]{1,0:T(8,128)(2,1)}) custom-call(bf16[384,512]{1,0:T(8,128)(2,1)} %get-tuple-element.4.mixer_in, bf16[384,512]{1,0:T(8,128)(2,1)} %bitcast.11), custom_call_target="tpu_custom_call" | custom-call | tf_op jit(solution)/shard_map/hand_over/pallas_call | solution.py:437

commit v4 on v3

--- a/solution.py
+++ b/solution.py
@@ -11,9 +11,10 @@
 EP = Z * PLANE
 CHIPS = Z * Y
 CAP = 24
-SEND = (0, 1, 7, 2, 6, 3, 5, 4)
+SEND = (1, 7, 2, 6, 0, 3, 5, 4)
 BACK = (4, 3, 5, 2, 6, 1, 7, 0)
-PAIR, DOWN = 6, 8
+EARLY = 4
+HALO = 8
 MESH = pl.DeviceIdType.MESH
 
 
@@ -35,10 +36,10 @@
     wi_hbm, wo_hbm, wv_hbm, wp_hbm, wg_hbm, wu_hbm, wd_hbm,
     mixer_out, expert_out,
     wi, wo, wv, wp, wg, wu, wd,
-    route, tok_send, tok, mrows, send, rows, hid, res, ret, gat, ext, ogate, acc, rim_s, rim_r, slot_rows, cols,
-    fin, fin_same, fin_pair,
+    route, tok_send, tok, mrows, halo, send, rows, hid, res, res_pair, ret, ret_pair, gat, ext, ogate, acc, slot_rows, cols,
+    fin, fin_same, fin_half, fin_pair,
     load_sem, wt_ss, wt_rs, route_ss, route_rs, tok_ss, tok_rs, mix_ss, mix_rs, disp_ss, disp_rs, row_ss, row_rs,
-    hid_ss, hid_rs, ret_ss, ret_rs, gat_ss, gat_rs, rim_ss, rim_rs, fin_ss, fin_rs,
+    hid_ss, hid_rs, ret_ss, ret_rs, gat_ss, gat_rs, halo_ss, halo_rs, fin_ss, fin_rs,
 ):
     ep, tp = lax.axis_index("ep"), lax.axis_index("tp")
     z, core = ep // PLANE, lax.rem(ep, C)
@@ -71,11 +72,20 @@
         pl.semaphore_signal(barrier, inc=1, device_id={"tp": other}, device_id_type=MESH)
         pl.semaphore_signal(barrier, inc=1, device_id={"ep": twin, "tp": other}, device_id_type=MESH)
 
+    @pl.when(tp != X - 1)
+    def _():
+        pl.semaphore_signal(
+            barrier, inc=1, device_id={"ep": lax.rem(ep + EP - 1, EP), "tp": X - 1}, device_id_type=MESH
+        )
+
     def to_ep(src, dst, ss, rs, target):
         return pltpu.make_async_remote_copy(src, dst, ss, rs, device_id={"ep": target}, device_id_type=MESH)
 
     def to_tp(src, dst, ss, rs, target):
         return pltpu.make_async_remote_copy(src, dst, ss, rs, device_id={"tp": target}, device_id_type=MESH)
+
+    def mixer_block(owner):
+        return mrows.at[owner]
 
     def to_twin(src, dst, ss, rs, target):
         return pltpu.make_async_remote_copy(
@@ -97,20 +107,33 @@
     for k in range(X):
         tok_send[k] = normed[:, k * 512 : (k + 1) * 512]
     tok[core, u] = tok_send[2 * u + core]
-    mrows[tp] = rms_rows(mixer_in[...], mixer_gain[...])
 
     for load in loads[:3]:
         load.wait()
-    pl.semaphore_wait(barrier, EP + 3)
+    half_a, half_b = pl.ds(0, 256), pl.ds(256, 256)
+    pl.semaphore_wait(barrier, EP + 3 + (X - 1) * (tp // (X - 1)))
 
     to_ep(route.at[core], route.at[core], route_ss, route_rs, twin).start()
     to_twin(tok_send.at[2 * (1 - u) + 1 - core], tok.at[core, u], tok_ss, tok_rs, mate).start()
     to_tp(tok_send.at[2 * (1 - u) + core], tok.at[core, u], tok_ss, tok_rs, mate).start()
     to_ep(tok_send.at[2 * u + 1 - core], tok.at[core, u], tok_ss, tok_rs, twin).start()
+    tail_rows = rms_rows(mixer_in[mixer_in.shape[0] - 16 :], mixer_gain[...])
+    halo[0] = tail_rows[16 - HALO :]
+
+    @pl.when(tp == X - 1)
+    def _():
+        for other in range(X):
+            pltpu.make_async_remote_copy(
+                halo.at[0], halo.at[1], halo_ss, halo_rs,
+                device_id={"ep": lax.rem(ep + 1, EP), "tp": other}, device_id_type=MESH,
+            ).start()
+
     to_tp(wg.at[0], wg.at[1], wt_ss.at[0], wt_rs.at[0], pair).start()
     to_tp(wu.at[0], wu.at[1], wt_ss.at[1], wt_rs.at[1], pair).start()
-    to_tp(mrows.at[tp], mrows.at[tp], mix_ss.at[0], mix_rs.at[0], pair).start()
-    to_tp(wd.at[0], wd.at[1], wt_ss.at[2], wt_rs.at[2], pair).start()
+    mrows[tp] = rms_rows(mixer_in[...], mixer_gain[...])
+    to_tp(mixer_block(tp), mixer_block(tp), mix_ss.at[0], mix_rs.at[0], pair).start()
+    to_tp(wd.at[0, :, half_a], wd.at[1, :, half_a], wt_ss.at[2], wt_rs.at[2], pair).start()
+    to_tp(wd.at[0, :, half_b], wd.at[1, :, half_b], wt_ss.at[3], wt_rs.at[3], pair).start()
 
     await_recv(route.at[1 - core], route_rs)
     lane = lax.broadcasted_iota(jnp.int32, (8, count), 1)
@@ -122,16 +145,13 @@
         lax.broadcasted_iota(jnp.int32, (count, count), 0) < lax.broadcasted_iota(jnp.int32, (count, count), 1)
     )
     earlier = jnp.dot(named, jnp.where(older, 1.0, 0.0).astype(jnp.bfloat16), preferred_element_type=jnp.float32)
-    total = both[2:3, :] + both[3:4, :]
     for k in range(2):
         within = jnp.sum(jnp.where(hot[k], earlier, 0.0), axis=0, keepdims=True)
         slot = both[k : k + 1, :] * CAP + within
         slot_rows[k : k + 1, :] = slot
-        cols[k] = jnp.transpose(jnp.broadcast_to(slot, (128, count)))
-        cols[2 + k] = jnp.transpose(jnp.broadcast_to(both[2 + k : 3 + k, :] / total, (128, count)))
 
     await_recv(send.at[pl.ds(0, 12)], tok_rs)
-    to_tp(mrows.at[tp], mrows.at[tp], mix_ss.at[1], mix_rs.at[1], mate).start()
+    to_tp(mixer_block(tp), mixer_block(tp), mix_ss.at[1], mix_rs.at[1], mate).start()
 
     @pl.loop(0, Z)
     def _(step):
@@ -157,6 +177,11 @@
             def _():
                 rows[2 * u + core, chip] = send[ep]
 
+    total = both[2:3, :] + both[3:4, :]
+    for k in range(2):
+        cols[k] = jnp.transpose(jnp.broadcast_to(slot_rows[k : k + 1, :], (128, count)))
+        cols[2 + k] = jnp.transpose(jnp.broadcast_to(both[2 + k : 3 + k, :] / total, (128, count)))
+
     def source_chips(offset):
         return pl.ds(lax.rem(z + Z - offset, Z) * Y, Y)
 
@@ -186,41 +211,83 @@
         hid[place, chips] = h.reshape(Y, CAP, 256).astype(jnp.bfloat16)
         to_tp(hid.at[place, chips], hid.at[place, chips], hid_ss, sem, mate).start()
 
-    def stage_down(step, which):
-        offset = pick_of((SEND, BACK)[which], step)
-        chips = source_chips(offset)
+    def down(chips, weight):
         out = None
         for k in range(X):
             h = hid[k, chips].reshape(Y * CAP, 256)
-            o = jnp.dot(h, wd[which, k * 256 : (k + 1) * 256, :], preferred_element_type=jnp.float32)
+            o = jnp.dot(h, weight(k), preferred_element_type=jnp.float32)
             out = o if k == 0 else out + o
-        res[which, chips] = out.reshape(Y, CAP, 512).astype(jnp.bfloat16)
+        return out.astype(jnp.bfloat16)
+
+    def stage_down(step):
+        offset = pick_of(SEND, step)
+        chips = source_chips(offset)
+        res[chips] = down(chips, lambda k: wd[0, k * 256 : (k + 1) * 256, :]).reshape(Y, CAP, 512)
 
         @pl.loop(0, Y)
         def _(j):
             goal = lax.rem(z + Z - offset, Z) * Y + j
-            target = goal * C + which
-
-            @pl.when(target != ep)
+
+            @pl.when(goal * C != ep)
             def _():
-                to_ep(res.at[which, goal], ret.at[ep], ret_ss.at[which], ret_rs.at[step], target).start()
-
-            @pl.when(target == ep)
+                to_ep(res.at[goal], ret.at[ep], ret_ss.at[0], ret_rs.at[0, step], goal * C).start()
+
+            @pl.when(goal * C == ep)
             def _():
-                ret[ep] = res[which, goal]
-
-    def stage_combine(step):
-        offset = jnp.where(core == 0, pick_of(SEND, step), pick_of(BACK, step))
-        plane = lax.rem(z + offset, Z)
-        await_slabs(ret_rs.at[step], offset == 0)
+                ret[ep] = res[goal]
+
+    def stage_down_pair(step, part):
+        offset = pick_of(BACK, step)
+        chips = source_chips(offset)
+        span = slice(part * 256, (part + 1) * 256)
+        res_pair[part, chips] = down(chips, lambda k: wd[1, k * 256 : (k + 1) * 256, span]).reshape(Y, CAP, 256)
+
+        @pl.loop(0, Y)
+        def _(j):
+            goal = lax.rem(z + Z - offset, Z) * Y + j
+            src, dst = res_pair.at[part, goal], ret_pair.at[part, ep]
+
+            @pl.when(goal * C + 1 != ep)
+            def _():
+                to_ep(src, dst, ret_ss.at[1 + part], ret_rs.at[1 + part, step], goal * C + 1).start()
+
+            @pl.when(goal * C + 1 == ep)
+            def _():
+                ret_pair[part, ep] = res_pair[part, goal]
+
+    def shares_of(plane):
         index = lax.broadcasted_iota(jnp.int32, (count, PLANE * CAP), 1) + plane * (PLANE * CAP)
         index = index.astype(jnp.float32)
         share = jnp.where(cols[0][:, 0:1] == index, cols[2][:, 0:1], 0.0)
         share = jnp.where(cols[1][:, 0:1] == index, cols[3][:, 0:1], share)
         high = share.astype(jnp.bfloat16)
-        low = (share - high.astype(jnp.float32)).astype(jnp.bfloat16)
+        return high, (share - high.astype(jnp.float32)).astype(jnp.bfloat16)
+
+    def stage_combine(step):
+        offset = pick_of(SEND, step)
+        plane = lax.rem(z + offset, Z)
+        await_slabs(ret_rs.at[0, step], offset == 0)
         got = ret[pl.ds(plane * PLANE, PLANE)].reshape(PLANE * CAP, 512)
+        high, low = shares_of(plane)
         acc[...] += jnp.dot(high, got, preferred_element_type=jnp.float32) + jnp.dot(
+            low, got, preferred_element_type=jnp.float32
+        )
+
+    def stage_combine_pair(step, part):
+        offset = pick_of(BACK, step)
+        plane = lax.rem(z + offset, Z)
+
+        @pl.when(offset == 0)
+        def _():
+            await_recv(ret_pair.at[part, pl.ds(0, PLANE - 1)], ret_rs.at[1 + part, step])
+
+        @pl.when(offset != 0)
+        def _():
+            await_recv(ret_pair.at[part, pl.ds(0, PLANE)], ret_rs.at[1 + part, step])
+
+        got = ret_pair[part, pl.ds(plane * PLANE, PLANE)].reshape(PLANE * CAP, 256)
+        high, low = shares_of(plane)
+        acc[:, part * 256 : (part + 1) * 256] += jnp.dot(high, got, preferred_element_type=jnp.float32) + jnp.dot(
             low, got, preferred_element_type=jnp.float32
         )
 
@@ -238,109 +305,121 @@
         chips = source_chips(pick_of(SEND, step))
         await_recv(hid.at[mate, chips], hid_rs.at[0, step])
         await_recv(hid.at[far, chips], hid_rs.at[1, step])
-        stage_down(step, 0)
-
-    @pl.loop(0, DOWN + Z // 2)
-    def _(s):
-        @pl.when(s < Z)
-        def _():
-            stage_rows(s)
-
-        @pl.when((s >= 1) & (s < Z + 1))
+        stage_down(step)
+
+    @pl.loop(0, Z - 1)
+    def _(s):
+        stage_rows(s)
+
+        @pl.when(s >= 1)
         def _():
             stage_own(s - 1)
 
-        @pl.when(s == PAIR)
-        def _():
-            await_recv(wg.at[1], wt_rs.at[0])
-            await_recv(wu.at[1], wt_rs.at[1])
-
-        @pl.when((s >= PAIR) & (s < PAIR + Z // 2))
-        def _():
-            stage_pair(2 * (s - PAIR))
-            stage_pair(2 * (s - PAIR) + 1)
-
-        @pl.when(s == PAIR + Z // 2)
-        def _():
-            await_recv(mrows.at[pair], mix_rs.at[0])
-            to_tp(mrows.at[pair], mrows.at[pair], mix_ss.at[2], mix_rs.at[2], mate).start()
-
-        @pl.when(s >= DOWN)
-        def _():
-            stage_down_own(2 * (s - DOWN))
-            stage_down_own(2 * (s - DOWN) + 1)
-
-    await_recv(mrows.at[mate], mix_rs.at[1])
+    await_recv(wg.at[1], wt_rs.at[0])
+    await_recv(wu.at[1], wt_rs.at[1])
+
+    @pl.loop(0, EARLY)
+    def _(s):
+        stage_pair(s)
+
+    stage_rows(Z - 1)
+    stage_own(Z - 2)
+
+    @pl.loop(EARLY, Z - 1)
+    def _(s):
+        stage_pair(s)
+
+    @pl.loop(0, EARLY)
+    def _(s):
+        stage_down_own(s)
+
+    stage_own(Z - 1)
+    stage_pair(Z - 1)
+    await_recv(mixer_block(pair), mix_rs.at[0])
+    to_tp(mixer_block(pair), mixer_block(pair), mix_ss.at[2], mix_rs.at[2], mate).start()
+
+    @pl.loop(EARLY, Z)
+    def _(s):
+        stage_down_own(s)
+
+    await_recv(wd.at[1, :, half_a], wt_rs.at[2])
+
+    @pl.loop(0, Z)
+    def _(s):
+        stage_down_pair(s, 0)
+
+    await_recv(halo.at[1], halo_rs)
+    await_recv(mixer_block(mate), mix_rs.at[1])
     for load in loads[3:]:
         load.wait()
-    await_recv(mrows.at[far], mix_rs.at[2])
-
-    @pl.loop(0, 2)
-    def _(n):
-        span = pl.ds(pl.multiple_of(n * 256, 256), 256)
-        m = mrows[...].reshape(count, 2048)
+    await_recv(mixer_block(far), mix_rs.at[2])
+
+    for n in range(2):
+        span = slice(n * 256, (n + 1) * 256)
+        m, before = mrows[...].reshape(count, 2048), halo[1]
         in_gate = jnp.dot(m, wi[:, span], preferred_element_type=jnp.float32)
         values = jnp.dot(m, wv[:, span], preferred_element_type=jnp.float32)
-        product = (in_gate * values).astype(jnp.bfloat16)
-        ext[8:, span] = product.astype(jnp.float32)
-        rim_s[:, span] = product[count - 16 :]
-        ogate[:, span] = jnp.dot(m, wo[:, span], preferred_element_type=jnp.float32)
-
-    to_ep(rim_s, rim_r, rim_ss, rim_rs, lax.rem(ep + 1, EP)).start()
-
-    await_recv(wd.at[1], wt_rs.at[2])
+        ext[HALO:, :] = (in_gate * values).astype(jnp.bfloat16).astype(jnp.float32)
+        in_gate = jnp.dot(before, wi[:, span], preferred_element_type=jnp.float32)
+        values = jnp.dot(before, wv[:, span], preferred_element_type=jnp.float32)
+        product = (in_gate * values).astype(jnp.bfloat16).astype(jnp.float32)
+        ext[0:HALO, :] = jnp.where(ep == 0, 0.0, product)
+        ogate[...] = jnp.dot(m, wo[:, span], preferred_element_type=jnp.float32)
+
+        for i in range(2):
+            lanes = slice(i * 128, (i + 1) * 128)
+            tap_span = pl.ds(pl.multiple_of(tp * 512 + n * 256 + i * 128, 128), 128)
+            conv = taps[0:1, tap_span] * ext[HALO - 2 : HALO - 2 + count, lanes]
+            conv = conv + taps[1:2, tap_span] * ext[HALO - 1 : HALO - 1 + count, lanes]
+            conv = conv + taps[2:3, tap_span] * ext[HALO:, lanes]
+            gat[tp, n, :, lanes] = (ogate[:, lanes] * conv).astype(jnp.bfloat16)
+
+        to_tp(gat.at[tp, n], gat.at[tp, n], gat_ss.at[0], gat_rs.at[0, n], pair).start()
+        to_tp(gat.at[tp, n], gat.at[tp, n], gat_ss.at[1], gat_rs.at[1, n], mate).start()
+
+    await_recv(wd.at[1, :, half_b], wt_rs.at[3])
 
     @pl.loop(0, Z)
     def _(s):
-        stage_down(s, 1)
-
-    await_recv(rim_r, rim_rs)
-    before = rim_r[...].astype(jnp.float32)[8:]
-    ext[0:8, :] = jnp.where(ep == 0, jnp.zeros_like(before), before)
-
-    @pl.loop(0, 4)
-    def _(n):
-        span = pl.ds(pl.multiple_of(n * 128, 128), 128)
-        tap_span = pl.ds(pl.multiple_of(tp * 512 + n * 128, 128), 128)
-        conv = taps[0:1, tap_span] * ext[6 : 6 + count, span]
-        conv = conv + taps[1:2, tap_span] * ext[7 : 7 + count, span]
-        conv = conv + taps[2:3, tap_span] * ext[8 : 8 + count, span]
-        gat[tp, :, span] = (ogate[:, span] * conv).astype(jnp.bfloat16)
-
-    to_tp(gat.at[tp], gat.at[tp], gat_ss.at[0], gat_rs.at[0], pair).start()
-    to_tp(gat.at[tp], gat.at[tp], gat_ss.at[1], gat_rs.at[1], mate).start()
-
-    @pl.loop(0, Z - 3)
-    def _(s):
-        stage_combine(s)
-
-    await_recv(gat.at[pair], gat_rs.at[0])
-    to_tp(gat.at[pair], gat.at[pair], gat_ss.at[2], gat_rs.at[2], mate).start()
-
-    @pl.loop(Z - 3, Z)
-    def _(s):
-        stage_combine(s)
-
-    fin[...] = acc[...].astype(jnp.bfloat16).reshape(C, count // 2, 512)
+        stage_down_pair(s, 1)
+
+    for n in range(2):
+        await_recv(gat.at[pair, n], gat_rs.at[0, n])
+        to_tp(gat.at[pair, n], gat.at[pair, n], gat_ss.at[2], gat_rs.at[2, n], mate).start()
 
     @pl.when(core == 0)
     def _():
+        @pl.loop(0, Z)
+        def _(s):
+            stage_combine(s)
+
+        fin[...] = acc[...].astype(jnp.bfloat16).reshape(C, count // 2, 512)
         to_ep(fin.at[1], fin_same, fin_ss.at[0], fin_rs.at[0], twin).start()
 
-    @pl.when(core == 1)
-    def _():
-        to_tp(fin.at[1], fin_pair, fin_ss.at[0], fin_rs.at[1], pair).start()
-        to_twin(fin.at[0], fin_pair, fin_ss.at[1], fin_rs.at[1], pair).start()
-
-    await_recv(gat.at[mate], gat_rs.at[1])
-    await_recv(gat.at[far], gat_rs.at[2])
+    def finish_pair(part):
+        @pl.when(core == 1)
+        def _():
+            @pl.loop(0, Z)
+            def _(s):
+                stage_combine_pair(s, part)
+
+            fin_half[part] = acc[:, part * 256 : (part + 1) * 256].astype(jnp.bfloat16).reshape(C, count // 2, 256)
+            to_tp(fin_half.at[part, 1], fin_pair.at[part], fin_ss.at[0], fin_rs.at[1 + part], pair).start()
+            to_twin(fin_half.at[part, 0], fin_pair.at[part], fin_ss.at[1], fin_rs.at[1 + part], pair).start()
+
+    finish_pair(0)
+    finish_pair(1)
+    for n in range(2):
+        await_recv(gat.at[mate, n], gat_rs.at[1, n])
+        await_recv(gat.at[far, n], gat_rs.at[2, n])
 
     @pl.loop(0, 2)
     def _(n):
         span = pl.ds(pl.multiple_of(n * 256, 256), 256)
         out = None
-        for k in range(X):
-            o = jnp.dot(gat[k], wp[k * 512 : (k + 1) * 512, span], preferred_element_type=jnp.float32)
+        for k in range(2 * X):
+            part = gat[k // 2, k % 2]
+            o = jnp.dot(part, wp[k * 256 : (k + 1) * 256, span], preferred_element_type=jnp.float32)
             out = o if k == 0 else out + o
         mixer_out[:, span] = out.astype(jnp.bfloat16)
 
@@ -357,33 +436,43 @@
         await_recv(fin_same, fin_rs.at[0])
         expert_out[first] = fin_same[0:own]
         expert_out[lax.rem(first + 1, X)] = fin_same[own:]
-        await_send(fin.at[1], fin_ss.at[0])
-        await_send(fin.at[0], fin_ss.at[1])
-
-    await_recv(fin_pair, fin_rs.at[1])
-    expert_out[lax.rem(first + 2, X)] = fin_pair[0:own]
-    expert_out[lax.rem(first + 3, X)] = fin_pair[own:]
+        await_send(fin_half.at[0], fin_ss.at[0])
+        await_send(fin_half.at[0], fin_ss.at[1])
+
+    for part in range(2):
+        await_recv(fin_pair.at[part], fin_rs.at[1 + part])
+        expert_out[lax.rem(first + 2, X), :, part * 256 : (part + 1) * 256] = fin_pair[part, 0:own]
+        expert_out[lax.rem(first + 3, X), :, part * 256 : (part + 1) * 256] = fin_pair[part, own:]
 
     await_send(route.at[0], route_ss)
     await_send(send.at[pl.ds(0, 12)], tok_ss)
-    await_send(rim_s, rim_ss)
-    for buf, sem in ((wg.at[0], wt_ss.at[0]), (wu.at[0], wt_ss.at[1]), (wd.at[0], wt_ss.at[2])):
-        await_send(buf, sem)
+    await_send(wg.at[0], wt_ss.at[0])
+    await_send(wu.at[0], wt_ss.at[1])
+    await_send(wd.at[0, :, half_a], wt_ss.at[2])
+    await_send(wd.at[0, :, half_b], wt_ss.at[3])
     for i in range(3):
-        await_send(mrows.at[0], mix_ss.at[i])
+        await_send(mixer_block(0), mix_ss.at[i])
         await_send(gat.at[0], gat_ss.at[i])
     await_send(send.at[pl.ds(0, EP - 1)], disp_ss)
     await_send(rows.at[pl.ds(0, 2)], row_ss)
     await_send(hid.at[pl.ds(0, 2)], hid_ss)
-    for which in range(C):
-
-        @pl.when(core == which)
-        def _():
-            await_send(ret.at[pl.ds(0, CHIPS - 1)], ret_ss.at[which])
-
-        @pl.when(core != which)
-        def _():
-            await_send(ret.at[pl.ds(0, CHIPS)], ret_ss.at[which])
+
+    @pl.when(tp == X - 1)
+    def _():
+        for _ in range(X):
+            await_send(halo.at[0], halo_ss)
+
+    @pl.when(core == 0)
+    def _():
+        await_send(ret.at[pl.ds(0, CHIPS - 1)], ret_ss.at[0])
+        await_send(ret_pair.at[0, pl.ds(0, CHIPS)], ret_ss.at[1])
+        await_send(ret_pair.at[0, pl.ds(0, CHIPS)], ret_ss.at[2])
+
+    @pl.when(core == 1)
+    def _():
+        await_send(ret.at[pl.ds(0, CHIPS)], ret_ss.at[0])
+        await_send(ret_pair.at[0, pl.ds(0, CHIPS - 1)], ret_ss.at[1])
+        await_send(ret_pair.at[0, pl.ds(0, CHIPS - 1)], ret_ss.at[2])
 
 
 def hand_over(mixer_in, expert_in, mixer_out, expert_out, held, in_sem, out_sem):
@@ -416,14 +505,17 @@
         out_specs=(local, local),
         scratch_shapes=[
             *[vmem((wide, 512), bf16)] * 4, *[vmem((2, wide, 256), bf16)] * 2, vmem((2, 1024, 512), bf16),
-            vmem((C, 8, count), f32), vmem((X, own, 512), bf16), vmem((C, 2, own, 512), bf16), vmem((X, own, wide), bf16),
+            vmem((C, 8, count), f32), vmem((X, own, 512), bf16), vmem((C, 2, own, 512), bf16),
+            vmem((X, own, wide), bf16), vmem((2, HALO, wide), bf16),
             vmem((EP, CAP, 512), bf16), vmem((X, CHIPS, CAP, 512), bf16), vmem((X, CHIPS, CAP, 256), bf16),
-            vmem((C, CHIPS, CAP, 512), bf16), vmem((EP, CAP, 512), bf16), vmem((X, count, 512), bf16),
-            vmem((count + 8, 512), f32), vmem((count, 512), f32), vmem((count, 512), f32),
-            vmem((16, 512), bf16), vmem((16, 512), bf16), vmem((8, count), f32), vmem((4, count, 128), f32),
-            vmem((C, count // 2, 512), bf16), vmem((count // 2, 512), bf16), vmem((count // 2, 512), bf16),
-            dma((7,)), dma((3,)), dma((3,)), dma, dma, dma, dma, dma((3,)), dma((3,)), dma, dma((Z,)), dma, dma((Z,)),
-            dma, dma((2, Z)), dma((2,)), dma((Z,)), dma((3,)), dma((3,)), dma, dma, dma((2,)), dma((2,)),
+            vmem((CHIPS, CAP, 512), bf16), vmem((2, CHIPS, CAP, 256), bf16),
+            vmem((EP, CAP, 512), bf16), vmem((2, EP, CAP, 256), bf16), vmem((X, 2, count, 256), bf16),
+            vmem((HALO + count, 256), f32), vmem((count, 256), f32), vmem((count, 512), f32),
+            vmem((8, count), f32), vmem((4, count, 128), f32),
+            vmem((C, count // 2, 512), bf16), vmem((count // 2, 512), bf16),
+            vmem((2, C, count // 2, 256), bf16), vmem((2, count // 2, 256), bf16),
+            dma((7,)), dma((4,)), dma((4,)), dma, dma, dma, dma, dma((3,)), dma((3,)), dma, dma((Z,)), dma, dma((Z,)),
+            dma, dma((2, Z)), dma((3,)), dma((3, Z)), dma((3,)), dma((3, 2)), dma, dma, dma((2,)), dma((3,)),
         ],
         compiler_params=pltpu.CompilerParams(
             collective_id=0, has_side_effects=True, vmem_limit_bytes=62 * 2**20

time: 126 us -> 119 us (0.944)
  Pallas kernels: 125 us -> 117 us
    pallas_call x1, Pallas kernels: 123 us -> 115 us  [on_device(): pl.pallas_call(kernel, out_shape=(out, jax.ShapeDtypeStruct((X, own, 512)...]
where the time goes in v4:
time: 119 us; the launch traced here: 117 us
  Pallas kernels  117 us (98%)
    pallas_call x1, Pallas kernels, on_device(): pl.pallas_call(kernel, out_shape=(out, jax.ShapeDtypeStruct((X, own, 512)...  115 us

profile of v4, /device:TPU:1, one launch (start us, length us, event | category | flops | bytes accessed | tf_op | source)
XLA Modules:
  0.0 117.3 jit_solution(9365370327021504316)
XLA Ops:
  0.6 114.8 %mixer_and_experts.1 = (bf16[384,512]{1,0:T(8,128)(2,1)}, bf16[4,96,512]{2,1,0:T(8,128)(2,1)}) custom-call(bf16[96,2048]{1,0:T(8,128)(2,1)} %mixer_in.1, bf16[96,2048]{1,0:T(8,128)(2,1)} %expert_in.1, f32[1,2048]{1,0:T(1,128)} %bitcast.12, f32[1,2048]{1,0:T(1,128)} %bitcast.13, f32[3,2048]{1,0:T(4,128)} %taps.1, s32[2,384]{1,0:T(2,128)} %bitcast.14, ...), custom_call_target="tpu_custom_call" | custom-call | tf_op jit(solution)/shard_map/mixer_and_experts/pallas_call | solution.py:501
  115.4 1.9 %hand_over.1 = (bf16[384,512]{1,0:T(8,128)(2,1)}, bf16[384,512]{1,0:T(8,128)(2,1)}) custom-call(bf16[384,512]{1,0:T(8,128)(2,1)} %get-tuple-element.4.mixer_in, bf16[384,512]{1,0:T(8,128)(2,1)} %bitcast.11), custom_call_target="tpu_custom_call" | custom-call | tf_op jit(solution)/shard_map/hand_over/pallas_call | solution.py:529

commit v5 on v4

--- a/solution.py
+++ b/solution.py
@@ -13,6 +13,7 @@
 CAP = 24
 SEND = (1, 7, 2, 6, 0, 3, 5, 4)
 BACK = (4, 3, 5, 2, 6, 1, 7, 0)
+SPANS = (slice(0, 256), slice(256, 512))
 EARLY = 4
 HALO = 8
 MESH = pl.DeviceIdType.MESH
@@ -36,12 +37,14 @@
     wi_hbm, wo_hbm, wv_hbm, wp_hbm, wg_hbm, wu_hbm, wd_hbm,
     mixer_out, expert_out,
     wi, wo, wv, wp, wg, wu, wd,
-    route, tok_send, tok, mrows, halo, send, rows, hid, res, res_pair, ret, ret_pair, gat, ext, ogate, acc, slot_rows, cols,
-    fin, fin_same, fin_half, fin_pair,
-    load_sem, wt_ss, wt_rs, route_ss, route_rs, tok_ss, tok_rs, mix_ss, mix_rs, disp_ss, disp_rs, row_ss, row_rs,
+    route, tok_send, tok, mrows, halo, send, rows, hid, res, res_pair_a, res_pair_b, ret, ret_pair_a, ret_pair_b, gat, ext, ogate, acc, slot_rows, cols,
+    fin, fin_same, fin_half_a, fin_half_b, fin_pair_a, fin_pair_b, picks_of, shares, mixed,
+    load_sem, store_sem, wt_ss, wt_rs, route_ss, route_rs, tok_ss, tok_rs, mix_ss, mix_rs, disp_ss, disp_rs, row_ss, row_rs,
     hid_ss, hid_rs, ret_ss, ret_rs, gat_ss, gat_rs, halo_ss, halo_rs, fin_ss, fin_rs,
 ):
     ep, tp = lax.axis_index("ep"), lax.axis_index("tp")
+    res_pair, ret_pair = (res_pair_a, res_pair_b), (ret_pair_a, ret_pair_b)
+    fin_half, fin_pair = (fin_half_a, fin_half_b), (fin_pair_a, fin_pair_b)
     z, core = ep // PLANE, lax.rem(ep, C)
     chip, twin = ep // C, ep + 1 - 2 * core
     odd = lax.rem(tp, 2)
@@ -110,7 +113,7 @@
 
     for load in loads[:3]:
         load.wait()
-    half_a, half_b = pl.ds(0, 256), pl.ds(256, 256)
+    half_a, half_b = (pl.ds(span.start, span.stop - span.start) for span in SPANS)
     pl.semaphore_wait(barrier, EP + 3 + (X - 1) * (tp // (X - 1)))
 
     to_ep(route.at[core], route.at[core], route_ss, route_rs, twin).start()
@@ -150,19 +153,19 @@
         slot = both[k : k + 1, :] * CAP + within
         slot_rows[k : k + 1, :] = slot
 
+    @pl.loop(0, Z)
+    def _(plane):
+        index = (lax.broadcasted_iota(jnp.int32, (PLANE * CAP, count), 0) + plane * (PLANE * CAP)).astype(jnp.float32)
+        pick = (index == slot_rows[0:1, :]) | (index == slot_rows[1:2, :])
+        picks_of[plane] = jnp.where(pick, 1.0, 0.0).astype(jnp.bfloat16)
+
     await_recv(send.at[pl.ds(0, 12)], tok_rs)
     to_tp(mixer_block(tp), mixer_block(tp), mix_ss.at[1], mix_rs.at[1], mate).start()
 
     @pl.loop(0, Z)
     def _(step):
         plane = lax.rem(z + pick_of(SEND, step), Z)
-        index = (lax.broadcasted_iota(jnp.int32, (PLANE * CAP, count), 0) + plane * (PLANE * CAP)).astype(jnp.float32)
-        pick = (index == slot_rows[0:1, :]) | (index == slot_rows[1:2, :])
-        moved = jnp.dot(
-            jnp.where(pick, 1.0, 0.0).astype(jnp.bfloat16),
-            tok[...].reshape(count, 512),
-            preferred_element_type=jnp.float32,
-        )
+        moved = jnp.dot(picks_of[plane], tok[...].reshape(count, 512), preferred_element_type=jnp.float32)
         send[pl.ds(plane * PLANE, PLANE)] = moved.reshape(PLANE, CAP, 512).astype(jnp.bfloat16)
 
         @pl.loop(0, PLANE)
@@ -239,39 +242,43 @@
     def stage_down_pair(step, part):
         offset = pick_of(BACK, step)
         chips = source_chips(offset)
-        span = slice(part * 256, (part + 1) * 256)
-        res_pair[part, chips] = down(chips, lambda k: wd[1, k * 256 : (k + 1) * 256, span]).reshape(Y, CAP, 256)
+        out = down(chips, lambda k: wd[1, k * 256 : (k + 1) * 256, SPANS[part]])
+        res_pair[part][chips] = out.reshape(Y, CAP, -1)
 
         @pl.loop(0, Y)
         def _(j):
             goal = lax.rem(z + Z - offset, Z) * Y + j
-            src, dst = res_pair.at[part, goal], ret_pair.at[part, ep]
 
             @pl.when(goal * C + 1 != ep)
             def _():
+                src, dst = res_pair[part].at[goal], ret_pair[part].at[ep]
                 to_ep(src, dst, ret_ss.at[1 + part], ret_rs.at[1 + part, step], goal * C + 1).start()
 
             @pl.when(goal * C + 1 == ep)
             def _():
-                ret_pair[part, ep] = res_pair[part, goal]
-
-    def shares_of(plane):
+                ret_pair[part][ep] = res_pair[part][goal]
+
+    @pl.loop(0, Z)
+    def _(plane):
         index = lax.broadcasted_iota(jnp.int32, (count, PLANE * CAP), 1) + plane * (PLANE * CAP)
         index = index.astype(jnp.float32)
         share = jnp.where(cols[0][:, 0:1] == index, cols[2][:, 0:1], 0.0)
         share = jnp.where(cols[1][:, 0:1] == index, cols[3][:, 0:1], share)
         high = share.astype(jnp.bfloat16)
-        return high, (share - high.astype(jnp.float32)).astype(jnp.bfloat16)
+        shares[0, plane] = high
+        shares[1, plane] = (share - high.astype(jnp.float32)).astype(jnp.bfloat16)
+
+    def weighted(plane, got):
+        return jnp.dot(shares[0, plane], got, preferred_element_type=jnp.float32) + jnp.dot(
+            shares[1, plane], got, preferred_element_type=jnp.float32
+        )
 
     def stage_combine(step):
         offset = pick_of(SEND, step)
         plane = lax.rem(z + offset, Z)
         await_slabs(ret_rs.at[0, step], offset == 0)
         got = ret[pl.ds(plane * PLANE, PLANE)].reshape(PLANE * CAP, 512)
-        high, low = shares_of(plane)
-        acc[...] += jnp.dot(high, got, preferred_element_type=jnp.float32) + jnp.dot(
-            low, got, preferred_element_type=jnp.float32
-        )
+        acc[...] += weighted(plane, got)
 
     def stage_combine_pair(step, part):
         offset = pick_of(BACK, step)
@@ -279,17 +286,14 @@
 
         @pl.when(offset == 0)
         def _():
-            await_recv(ret_pair.at[part, pl.ds(0, PLANE - 1)], ret_rs.at[1 + part, step])
+            await_recv(ret_pair[part].at[pl.ds(0, PLANE - 1)], ret_rs.at[1 + part, step])
 
         @pl.when(offset != 0)
         def _():
-            await_recv(ret_pair.at[part, pl.ds(0, PLANE)], ret_rs.at[1 + part, step])
-
-        got = ret_pair[part, pl.ds(plane * PLANE, PLANE)].reshape(PLANE * CAP, 256)
-        high, low = shares_of(plane)
-        acc[:, part * 256 : (part + 1) * 256] += jnp.dot(high, got, preferred_element_type=jnp.float32) + jnp.dot(
-            low, got, preferred_element_type=jnp.float32
-        )
+            await_recv(ret_pair[part].at[pl.ds(0, PLANE)], ret_rs.at[1 + part, step])
+
+        got = ret_pair[part][pl.ds(plane * PLANE, PLANE)].reshape(PLANE * CAP, -1)
+        acc[:, SPANS[part]] += weighted(plane, got)
 
     acc[...] = jnp.zeros(acc.shape, jnp.float32)
 
@@ -348,31 +352,39 @@
     def _(s):
         stage_down_pair(s, 0)
 
-    await_recv(halo.at[1], halo_rs)
-    await_recv(mixer_block(mate), mix_rs.at[1])
+    def stage_mixer(block):
+        m = mrows[block]
+        at = pl.multiple_of(block * m.shape[0], 16)
+        in_gate = jnp.dot(m, wi[...], preferred_element_type=jnp.float32)
+        values = jnp.dot(m, wv[...], preferred_element_type=jnp.float32)
+        ext[pl.ds(HALO + at, m.shape[0]), :] = (in_gate * values).astype(jnp.bfloat16).astype(jnp.float32)
+        ogate[pl.ds(at, m.shape[0]), :] = jnp.dot(m, wo[...], preferred_element_type=jnp.float32)
+
     for load in loads[3:]:
         load.wait()
-    await_recv(mixer_block(far), mix_rs.at[2])
+    await_recv(halo.at[1], halo_rs)
+    in_gate = jnp.dot(halo[1], wi[...], preferred_element_type=jnp.float32)
+    values = jnp.dot(halo[1], wv[...], preferred_element_type=jnp.float32)
+    product = (in_gate * values).astype(jnp.bfloat16).astype(jnp.float32)
+    ext[0:HALO, :] = jnp.where(ep == 0, 0.0, product)
+    await_recv(mixer_block(mate), mix_rs.at[1])
+
+    @pl.loop(0, X)
+    def _(n):
+        @pl.when(n == X - 1)
+        def _():
+            await_recv(mixer_block(far), mix_rs.at[2])
+
+        stage_mixer(jnp.where(n == X - 1, far, jnp.where(n == 0, tp, jnp.where(n == 1, mate, pair))))
 
     for n in range(2):
-        span = slice(n * 256, (n + 1) * 256)
-        m, before = mrows[...].reshape(count, 2048), halo[1]
-        in_gate = jnp.dot(m, wi[:, span], preferred_element_type=jnp.float32)
-        values = jnp.dot(m, wv[:, span], preferred_element_type=jnp.float32)
-        ext[HALO:, :] = (in_gate * values).astype(jnp.bfloat16).astype(jnp.float32)
-        in_gate = jnp.dot(before, wi[:, span], preferred_element_type=jnp.float32)
-        values = jnp.dot(before, wv[:, span], preferred_element_type=jnp.float32)
-        product = (in_gate * values).astype(jnp.bfloat16).astype(jnp.float32)
-        ext[0:HALO, :] = jnp.where(ep == 0, 0.0, product)
-        ogate[...] = jnp.dot(m, wo[:, span], preferred_element_type=jnp.float32)
-
         for i in range(2):
-            lanes = slice(i * 128, (i + 1) * 128)
+            lanes = slice(n * 256 + i * 128, n * 256 + (i + 1) * 128)
             tap_span = pl.ds(pl.multiple_of(tp * 512 + n * 256 + i * 128, 128), 128)
             conv = taps[0:1, tap_span] * ext[HALO - 2 : HALO - 2 + count, lanes]
             conv = conv + taps[1:2, tap_span] * ext[HALO - 1 : HALO - 1 + count, lanes]
             conv = conv + taps[2:3, tap_span] * ext[HALO:, lanes]
-            gat[tp, n, :, lanes] = (ogate[:, lanes] * conv).astype(jnp.bfloat16)
+            gat[tp, n, :, i * 128 : (i + 1) * 128] = (ogate[:, lanes] * conv).astype(jnp.bfloat16)
 
         to_tp(gat.at[tp, n], gat.at[tp, n], gat_ss.at[0], gat_rs.at[0, n], pair).start()
         to_tp(gat.at[tp, n], gat.at[tp, n], gat_ss.at[1], gat_rs.at[1, n], mate).start()
@@ -383,9 +395,11 @@
     def _(s):
         stage_down_pair(s, 1)
 
-    for n in range(2):
+    def gated_pass(n):
         await_recv(gat.at[pair, n], gat_rs.at[0, n])
         to_tp(gat.at[pair, n], gat.at[pair, n], gat_ss.at[2], gat_rs.at[2, n], mate).start()
+
+    gated_pass(0)
 
     @pl.when(core == 0)
     def _():
@@ -396,18 +410,26 @@
         fin[...] = acc[...].astype(jnp.bfloat16).reshape(C, count // 2, 512)
         to_ep(fin.at[1], fin_same, fin_ss.at[0], fin_rs.at[0], twin).start()
 
+    def combine_pair(part, start, stop):
+        @pl.when(core == 1)
+        def _():
+            @pl.loop(start, stop)
+            def _(s):
+                stage_combine_pair(s, part)
+
     def finish_pair(part):
         @pl.when(core == 1)
         def _():
-            @pl.loop(0, Z)
-            def _(s):
-                stage_combine_pair(s, part)
-
-            fin_half[part] = acc[:, part * 256 : (part + 1) * 256].astype(jnp.bfloat16).reshape(C, count // 2, 256)
-            to_tp(fin_half.at[part, 1], fin_pair.at[part], fin_ss.at[0], fin_rs.at[1 + part], pair).start()
-            to_twin(fin_half.at[part, 0], fin_pair.at[part], fin_ss.at[1], fin_rs.at[1 + part], pair).start()
-
+            fin_half[part][...] = acc[:, SPANS[part]].astype(jnp.bfloat16).reshape(C, count // 2, -1)
+            out, into = fin_half[part], fin_pair[part]
+            to_twin(out.at[0], into, fin_ss.at[1 + part], fin_rs.at[1 + part], pair).start()
+            to_tp(out.at[1], into, fin_ss.at[3 + part], fin_rs.at[1 + part], pair).start()
+
+    combine_pair(0, 0, 4)
+    gated_pass(1)
+    combine_pair(0, 4, Z)
     finish_pair(0)
+    combine_pair(1, 0, Z)
     finish_pair(1)
     for n in range(2):
         await_recv(gat.at[mate, n], gat_rs.at[1, n])
@@ -421,28 +443,45 @@
             part = gat[k // 2, k % 2]
             o = jnp.dot(part, wp[k * 256 : (k + 1) * 256, span], preferred_element_type=jnp.float32)
             out = o if k == 0 else out + o
-        mixer_out[:, span] = out.astype(jnp.bfloat16)
+        mixed[:, span] = out.astype(jnp.bfloat16)
+
+    stores = [pltpu.make_async_copy(mixed, mixer_out, store_sem.at[0])]
+    stores[0].start()
 
     own = count // 4
 
+    def store_rows(src, block, span, at):
+        for place in range(2):
+            copy = pltpu.make_async_copy(
+                src.at[pl.ds(place * own, own)],
+                expert_out.at[lax.rem(first + block + place, X), :, span],
+                store_sem.at[at + place],
+            )
+            copy.start()
+            stores.append(copy)
+
+    @pl.when(core == 1)
+    def _():
+        await_recv(fin_same, fin_rs.at[0])
+        fin[0] = fin_same[...]
+
+    store_rows(fin.at[0], 0, slice(None), 1)
+    for part in range(2):
+        await_recv(fin_pair[part], fin_rs.at[1 + part])
+        store_rows(fin_pair[part], 2, SPANS[part], 3 + 2 * part)
+
+    for copy in stores:
+        copy.wait()
+
     @pl.when(core == 0)
     def _():
-        expert_out[first] = fin[0, 0:own]
-        expert_out[lax.rem(first + 1, X)] = fin[0, own:]
         await_send(fin.at[1], fin_ss.at[0])
 
     @pl.when(core == 1)
     def _():
-        await_recv(fin_same, fin_rs.at[0])
-        expert_out[first] = fin_same[0:own]
-        expert_out[lax.rem(first + 1, X)] = fin_same[own:]
-        await_send(fin_half.at[0], fin_ss.at[0])
-        await_send(fin_half.at[0], fin_ss.at[1])
-
-    for part in range(2):
-        await_recv(fin_pair.at[part], fin_rs.at[1 + part])
-        expert_out[lax.rem(first + 2, X), :, part * 256 : (part + 1) * 256] = fin_pair[part, 0:own]
-        expert_out[lax.rem(first + 3, X), :, part * 256 : (part + 1) * 256] = fin_pair[part, own:]
+        for part in range(2):
+            await_send(fin_pair[part], fin_ss.at[1 + part])
+            await_send(fin_pair[part], fin_ss.at[3 + part])
 
     await_send(route.at[0], route_ss)
     await_send(send.at[pl.ds(0, 12)], tok_ss)
@@ -465,14 +504,14 @@
     @pl.when(core == 0)
     def _():
         await_send(ret.at[pl.ds(0, CHIPS - 1)], ret_ss.at[0])
-        await_send(ret_pair.at[0, pl.ds(0, CHIPS)], ret_ss.at[1])
-        await_send(ret_pair.at[0, pl.ds(0, CHIPS)], ret_ss.at[2])
+        await_send(ret_pair[0].at[pl.ds(0, CHIPS)], ret_ss.at[1])
+        await_send(ret_pair[1].at[pl.ds(0, CHIPS)], ret_ss.at[2])
 
     @pl.when(core == 1)
     def _():
         await_send(ret.at[pl.ds(0, CHIPS)], ret_ss.at[0])
-        await_send(ret_pair.at[0, pl.ds(0, CHIPS - 1)], ret_ss.at[1])
-        await_send(ret_pair.at[0, pl.ds(0, CHIPS - 1)], ret_ss.at[2])
+        await_send(ret_pair[0].at[pl.ds(0, CHIPS - 1)], ret_ss.at[1])
+        await_send(ret_pair[1].at[pl.ds(0, CHIPS - 1)], ret_ss.at[2])
 
 
 def hand_over(mixer_in, expert_in, mixer_out, expert_out, held, in_sem, out_sem):
@@ -493,6 +532,7 @@
 ):
     bf16, f32 = jnp.bfloat16, jnp.float32
     own, wide = mixer_in.shape
+    parts = [span.stop - span.start for span in SPANS]
     count = route_ids.shape[0]
     local = pl.BlockSpec(memory_space=pltpu.VMEM)
     remote = pl.BlockSpec(memory_space=pl.ANY)
@@ -502,20 +542,21 @@
         kernel,
         out_shape=(out, jax.ShapeDtypeStruct((X, own, 512), bf16)),
         in_specs=[local] * 7 + [remote] * 7,
-        out_specs=(local, local),
+        out_specs=(remote, remote),
         scratch_shapes=[
             *[vmem((wide, 512), bf16)] * 4, *[vmem((2, wide, 256), bf16)] * 2, vmem((2, 1024, 512), bf16),
             vmem((C, 8, count), f32), vmem((X, own, 512), bf16), vmem((C, 2, own, 512), bf16),
             vmem((X, own, wide), bf16), vmem((2, HALO, wide), bf16),
             vmem((EP, CAP, 512), bf16), vmem((X, CHIPS, CAP, 512), bf16), vmem((X, CHIPS, CAP, 256), bf16),
-            vmem((CHIPS, CAP, 512), bf16), vmem((2, CHIPS, CAP, 256), bf16),
-            vmem((EP, CAP, 512), bf16), vmem((2, EP, CAP, 256), bf16), vmem((X, 2, count, 256), bf16),
-            vmem((HALO + count, 256), f32), vmem((count, 256), f32), vmem((count, 512), f32),
+            vmem((CHIPS, CAP, 512), bf16), *[vmem((CHIPS, CAP, part), bf16) for part in parts],
+            vmem((EP, CAP, 512), bf16), *[vmem((EP, CAP, part), bf16) for part in parts], vmem((X, 2, count, 256), bf16),
+            vmem((HALO + count, 512), f32), vmem((count, 512), f32), vmem((count, 512), f32),
             vmem((8, count), f32), vmem((4, count, 128), f32),
             vmem((C, count // 2, 512), bf16), vmem((count // 2, 512), bf16),
-            vmem((2, C, count // 2, 256), bf16), vmem((2, count // 2, 256), bf16),
-            dma((7,)), dma((4,)), dma((4,)), dma, dma, dma, dma, dma((3,)), dma((3,)), dma, dma((Z,)), dma, dma((Z,)),
-            dma, dma((2, Z)), dma((3,)), dma((3, Z)), dma((3,)), dma((3, 2)), dma, dma, dma((2,)), dma((3,)),
+            *[vmem((C, count // 2, part), bf16) for part in parts], *[vmem((count // 2, part), bf16) for part in parts],
+            vmem((Z, PLANE * CAP, count), bf16), vmem((2, Z, count, PLANE * CAP), bf16), vmem((count, 512), bf16),
+            dma((7,)), dma((7,)), dma((4,)), dma((4,)), dma, dma, dma, dma, dma((3,)), dma((3,)), dma, dma((Z,)), dma, dma((Z,)),
+            dma, dma((2, Z)), dma((3,)), dma((3, Z)), dma((3,)), dma((3, 2)), dma, dma, dma((5,)), dma((3,)),
         ],
         compiler_params=pltpu.CompilerParams(
             collective_id=0, has_side_effects=True, vmem_limit_bytes=62 * 2**20

time: 119 us -> 118 us (level)
  no operation moved by 1% of the time
where the time goes in v5:
time: 118 us; the launch traced here: 117 us
  Pallas kernels  117 us (99%)
    pallas_call x1, Pallas kernels, on_device(): pl.pallas_call(kernel, out_shape=(out, jax.ShapeDtypeStruct((X, own, 512)...  115 us

profile of v5, /device:TPU:1, one launch (start us, length us, event | category | flops | bytes accessed | tf_op | source)
XLA Modules:
  0.0 117.2 jit_solution(3692315917738671819)
XLA Ops:
  0.6 114.7 %mixer_and_experts.1 = (bf16[384,512]{1,0:T(8,128)(2,1)}, bf16[4,96,512]{2,1,0:T(8,128)(2,1)}) custom-call(bf16[96,2048]{1,0:T(8,128)(2,1)} %mixer_in.1, bf16[96,2048]{1,0:T(8,128)(2,1)} %expert_in.1, f32[1,2048]{1,0:T(1,128)} %bitcast.12, f32[1,2048]{1,0:T(1,128)} %bitcast.13, f32[3,2048]{1,0:T(4,128)} %taps.1, s32[2,384]{1,0:T(2,128)} %bitcast.14, ...), custom_call_target="tpu_custom_call" | custom-call | tf_op jit(solution)/shard_map/mixer_and_experts/pallas_call | solution.py:541
  115.3 1.9 %hand_over.1 = (bf16[384,512]{1,0:T(8,128)(2,1)}, bf16[384,512]{1,0:T(8,128)(2,1)}) custom-call(bf16[384,512]{1,0:T(8,128)(2,1)} %get-tuple-element.4.mixer_in, bf16[384,512]{1,0:T(8,128)(2,1)} %bitcast.11), custom_call_target="tpu_custom_call" | custom-call | tf_op jit(solution)/shard_map/hand_over/pallas_call | solution.py:570

commit v6 on v5

--- a/solution.py
+++ b/solution.py
@@ -415,7 +415,7 @@
         def _():
             @pl.loop(start, stop)
             def _(s):
-                stage_combine_pair(s, part)
+                stage_combine_pair(jnp.where(s == 0, 0, jnp.where(s == Z - 1, 1, s + 1)), part)
 
     def finish_pair(part):
         @pl.when(core == 1)

time: 118 us -> 119 us (level)
  no operation moved by 1% of the time
where the time goes in v6:
time: 119 us; the launch traced here: 117 us
  Pallas kernels  117 us (98%)
    pallas_call x1, Pallas kernels, on_device(): pl.pallas_call(kernel, out_shape=(out, jax.ShapeDtypeStruct((X, own, 512)...  115 us

profile of v6, /device:TPU:1, one launch (start us, length us, event | category | flops | bytes accessed | tf_op | source)
XLA Modules:
  0.0 117.5 jit_solution(16179066838996225082)
XLA Ops:
  0.6 114.9 %mixer_and_experts.1 = (bf16[384,512]{1,0:T(8,128)(2,1)}, bf16[4,96,512]{2,1,0:T(8,128)(2,1)}) custom-call(bf16[96,2048]{1,0:T(8,128)(2,1)} %mixer_in.1, bf16[96,2048]{1,0:T(8,128)(2,1)} %expert_in.1, f32[1,2048]{1,0:T(1,128)} %bitcast.12, f32[1,2048]{1,0:T(1,128)} %bitcast.13, f32[3,2048]{1,0:T(4,128)} %taps.1, s32[2,384]{1,0:T(2,128)} %bitcast.14, ...), custom_call_target="tpu_custom_call" | custom-call | tf_op jit(solution)/shard_map/mixer_and_experts/pallas_call | solution.py:541
  115.6 1.9 %hand_over.1 = (bf16[384,512]{1,0:T(8,128)(2,1)}, bf16[384,512]{1,0:T(8,128)(2,1)}) custom-call(bf16[384,512]{1,0:T(8,128)(2,1)} %get-tuple-element.4.mixer_in, bf16[384,512]{1,0:T(8,128)(2,1)} %bitcast.11), custom_call_target="tpu_custom_call" | custom-call | tf_op jit(solution)/shard_map/hand_over/pallas_call | solution.py:570
